TPU v7x, 32 devices: a whole 2x2x4 slice. The times are simulated.
32 devices in a mesh: ep: 8 (over z, x), tp: 4 (over y, core).
Axes of the slice: x: 2, y: 2, z: 4, core: 2. Of those that a mesh axis runs over, the one named last changes fastest.
Arguments:
- mixer_rows: bfloat16 [2048, 4096], P('ep'), may hold values from -8 to 8, as said below
- mixer_gain: float32 [4096], replicated, may hold values from 0.1 to 1.9
- gate_proj: bfloat16 [4096, 4096], P(None, 'tp'), may hold values from -0.09375 to 0.09375
- input_proj: bfloat16 [4096, 4096], P(None, 'tp'), may hold values from -0.09375 to 0.09375
- conv_taps: float32 [4, 4096], P(None, 'tp'), may hold values from -2 to 2
- input_gates: bfloat16 [16, 256, 256], P('tp'), may hold values from -0.375 to 0.375
- decay_gates: bfloat16 [16, 256, 256], P('tp'), may hold values from -0.375 to 0.375
- decay_offset: float32 [4096], P('tp'), may hold values from 4.8 to 13, as said below
- out_proj: bfloat16 [4096, 4096], P('tp'), may hold values from -0.09375 to 0.09375
- mixer_scale: float32 [4096], replicated, may hold values from 0.1 to 1.9
- expert_rows: bfloat16 [2048, 4096], P('ep'), may hold values from -6 to 6
- expert_gain: float32 [4096], replicated, may hold values from 0.1 to 1.9
- route_ids: int32 [2048, 2], P('ep'), may hold values from 0 to 7, all different within a row; in each aligned block of 256 rows (0 to 255, 256 to 511, ...) at most 96 rows name the same one
- route_weights: float32 [2048, 2], P('ep'), may hold values from 0.5 to 2
- expert_gate: bfloat16 [8, 4096, 1024], P('ep', None, 'tp'), may hold values from -0.09375 to 0.09375
- expert_up: bfloat16 [8, 4096, 1024], P('ep', None, 'tp'), may hold values from -0.09375 to 0.09375
- expert_down: bfloat16 [8, 1024, 4096], P('ep', 'tp'), may hold values from -0.1875 to 0.1875
- shared_gate: bfloat16 [4096, 1024], P(None, 'tp'), may hold values from -0.09375 to 0.09375
- shared_up: bfloat16 [4096, 1024], P(None, 'tp'), may hold values from -0.09375 to 0.09375
- shared_down: bfloat16 [1024, 4096], P('tp'), may hold values from -0.1875 to 0.1875
- expert_scale: float32 [4096], replicated, may hold values from 0.1 to 1.9
Outputs:
- mixer_out: bfloat16 [2048, 4096], P(('ep', 'tp'))
- expert_out: bfloat16 [2048, 4096], P(('ep', 'tp'))
Inputs may be any that keep to these rules, and one draw needn't show every extreme that they name: `mixer_rows`: order one, with a common direction whose weight drifts slowly along the sequence. `decay_offset`: the even channels forget within some 30 to 200 tokens; the odd channels keep 5 to 90 percent of their state over the whole sequence of 2048 tokens. `route_ids`: each row names 2 different experts; within the rows of one index of ep (aligned blocks of 256 rows) no expert is named by more than 96 rows, and in some blocks one is named by exactly 96.
All inputs are finite; a program needn't handle non-finite values.
Results may differ from a plain program's by a relative error of at most 0.0033.
The roundings to bfloat16 on the way count: a program that leaves them out, or rounds other values in their place, can miss the bound.
Values may be sent and summed in bfloat16 or wider, within the bound.
A program may use at most 192 MiB of HBM per device.

v0:
```python
import functools

import jax
import jax.numpy as jnp
from jax import lax
from jax.experimental import pallas as pl
from jax.experimental.pallas import tpu as pltpu
from jax.sharding import PartitionSpec as P

eps = 1e-06
lru_power = 8.0
halo_rows = 16
MESH = pl.DeviceIdType.MESH
f32 = jnp.float32
bf16 = jnp.bfloat16


def rms_scale(values, scale):
    floats = values.astype(f32)
    return floats * lax.rsqrt(jnp.mean(floats * floats, axis=-1, keepdims=True) + eps) * scale


def remote(src, dst, send_sem, recv_sem, ep_at, tp_at):
    return pltpu.make_async_remote_copy(
        src_ref=src,
        dst_ref=dst,
        send_sem=send_sem,
        recv_sem=recv_sem,
        device_id=(ep_at, tp_at),
        device_id_type=MESH,
    )


def greet(peers):
    barrier = pltpu.get_barrier_semaphore()
    for ep_at, tp_at in peers:
        pl.semaphore_signal(barrier, inc=1, device_id=(ep_at, tp_at), device_id_type=MESH)
    pl.semaphore_wait(barrier, len(peers))


def expm1_neg(y):
    series = y * (1 + y / 2 * (1 + y / 3 * (1 + y / 4 * (1 + y / 5 * (1 + y / 6 * (1 + y / 7))))))
    return jnp.where(y > -0.35, series, jnp.exp(y) - 1.0)


def layer_kernel(
    ep, tp, top,
    slots, slots_t, taps_ref, ig_ref, dg_ref, soft_ref, weights, mg_ref, xg_ref, ms_ref, es_ref,
    rows_hbm, tokens_hbm, ip_hbm, gp_hbm, op_hbm, eg_hbm, eu_hbm, ed, sg_hbm, su_hbm, sd_hbm,
    mo_ref, eo_ref,
    outq, normed, en, e_out, r_out, r_near,
    w1, eg, eu, wd, sd, recv, hid, ret, back, mt, st, m_half, e_half, m_out, m_in, e_in,
    r_buf, r_in, total, gate, a_buf, b_buf, ext, tail, halo, ends, got, gated,
    load_sem, halo_send, halo_recv, end_send, end_recv,
    z_s, z_r, y_s, y_r, c_s, c_r, hy_s, hy_r, hc_s, hc_r, w_s, w_r, b_s, b_r,
    md_s, md_r, ed_s, ed_r, my_s, my_r, ey_s, ey_r, r_s, r_r,
):
    me, t = lax.axis_index("ep"), lax.axis_index("tp")
    ys = tp // 2
    y, c = t // 2, lax.rem(t, 2)
    mate = y * 2 + 1 - c
    dq = outq.shape[2]
    rows, width = ext.shape[0] - halo_rows, ext.shape[1]
    each = rows // tp
    blocks, bw = ig_ref.shape[0], ig_ref.shape[1]
    sh_width = sd.shape[0]

    def at_y(k):
        return lax.rem(y + k, ys)

    def up(k):
        return at_y(k) * 2 + c

    def down_of(k, core):
        return lax.rem(y + ys - k, ys) * 2 + core

    greet(
        [(lax.rem(me + i, ep), t) for i in range(1, ep)]
        + [(me, lax.rem(t + i, tp)) for i in range(1, tp)]
    )

    def z_copy(i):
        return remote(
            outq.at[i], recv.at[t, i], z_s.at[i], z_r.at[i], lax.rem(me + i, ep), t
        )

    def y_copy(k, i):
        return remote(recv.at[t, i], recv.at[t, i], y_s.at[k, i], y_r.at[k, i], me, up(k))

    def c_copy(k, i):
        q = down_of(k, c)
        return remote(recv.at[q, i], recv.at[q, i], c_s.at[k, i], c_r.at[k, i], me, mate)

    def hy_copy(k, i):
        return remote(hid.at[t, i], hid.at[t, i], hy_s.at[k, i], hy_r.at[k, i], me, up(k))

    def hc_copy(k, i):
        q = down_of(k, c)
        return remote(hid.at[q, i], hid.at[q, i], hc_s.at[k, i], hc_r.at[k, i], me, mate)

    def w_copy(i):
        q = lax.rem(t + i, tp)
        return remote(
            ed.at[:, pl.ds(pl.multiple_of(q * dq, dq), dq)], wd.at[t],
            w_s.at[i], w_r.at[i], me, q,
        )

    def b_copy(i):
        return remote(
            ret.at[i], back.at[i], b_s.at[i], b_r.at[i], lax.rem(me + ep - i, ep), t
        )

    def halo_copy():
        return remote(tail, halo, halo_send, halo_recv, lax.rem(me + 1, ep), t)

    def end_copy(i):
        return remote(ends, got.at[i], end_send.at[i], end_recv.at[i], lax.rem(me + i, ep), t)

    def pair(ref, half, s, r, k):
        return remote(ref.at[at_y(k) * 2 + 1 - c], half.at[k], s.at[k], r.at[k], me, mate)

    def my_copy(k):
        return remote(m_out.at[k], m_in.at[k], my_s.at[k], my_r.at[k], me, up(k))

    def ey_copy(k):
        return remote(e_out.at[k], e_in.at[k], ey_s.at[k], ey_r.at[k], me, up(k))

    def r_copy(k, core):
        j, q = 2 * k + core, at_y(k) * 2 + lax.rem(c + core, 2)
        if k == 0:
            return remote(r_buf.at[q], r_near, r_s.at[j], r_r.at[j], me, q)
        return remote(r_out.at[q], r_in.at[t], r_s.at[j], r_r.at[j], me, q)

    def load(src, dst, at):
        return pltpu.make_async_copy(src, dst, load_sem.at[at])

    for i in range(1, tp):
        w_copy(i).start()
    tokens_load, rows_load = load(tokens_hbm, en, 0), load(rows_hbm, normed, 9 + tp)
    tokens_load.start()
    rows_load.start()
    ip_load = load(ip_hbm, w1, 1)
    ip_load.start()
    eg_load, eu_load = load(eg_hbm, eg, 2), load(eu_hbm, eu, 3)
    eg_load.start()
    eu_load.start()
    wd_load = load(ed.at[:, pl.ds(pl.multiple_of(t * dq, dq), dq)], wd.at[t], 4)
    wd_load.start()
    sd_load = load(sd_hbm, sd, 5)
    sd_load.start()

    def normalize(ref, gain):
        def some(r, _):
            at = pl.ds(pl.multiple_of(r * 32, 32), 32)
            ref[at, :] = rms_scale(ref[at, :], gain[...]).astype(bf16)
            return 0

        lax.fori_loop(0, rows // 32, some, 0)

    tokens_load.wait()
    normalize(en, xg_ref)
    cap = outq.shape[1]
    mine = pl.ds(pl.multiple_of(t * dq, dq), dq)

    def place(i):
        spot = lax.broadcasted_iota(jnp.int32, (cap, rows), 0) + i * cap
        hot = slots_t[0:1, :] == spot
        for k in range(1, top):
            hot = hot | (slots_t[k : k + 1, :] == spot)
        return hot.astype(f32).astype(bf16)

    def dispatch(i, _):
        outq[i] = jnp.dot(place(i), en[:, mine], preferred_element_type=f32).astype(bf16)
        z_copy(i).start()
        return 0

    lax.fori_loop(1, ep, dispatch, 0)
    local = place(0)
    for q in range(tp):
        recv[q, 0] = jnp.dot(
            local, en[:, pl.ds(q * dq, dq)], preferred_element_type=f32
        ).astype(bf16)
    rows_load.wait()
    normalize(normed, mg_ref)
    sg_load = load(sg_hbm, w1.at[:, pl.ds(0, sh_width)], 6)
    su_load = load(su_hbm, w1.at[:, pl.ds(sh_width, sh_width)], 7)
    gp_load = load(gp_hbm, w1, 8)
    op_loads = [
        load(op_hbm.at[:, pl.ds(q * dq, dq)], w1.at[pl.ds(q * width, width), :], 9 + q)
        for q in range(tp)
    ]

    def project():
        ip_load.wait()

        def columns(j, _):
            cols = pl.ds(pl.multiple_of(j * bw, bw), bw)
            piece = jnp.dot(normed[...], w1[:, cols], preferred_element_type=f32).astype(bf16)
            ext[pl.ds(halo_rows, rows), cols] = piece.astype(f32)
            tail[:, cols] = piece[rows - halo_rows :]
            return 0

        lax.fori_loop(0, width // bw, columns, 0)
        halo_copy().start()
        sg_load.start()
        su_load.start()

    def shared():
        sg_load.wait()
        su_load.wait()
        g = jnp.dot(en[...], w1[:, pl.ds(0, sh_width)], preferred_element_type=f32)
        u = jnp.dot(en[...], w1[:, pl.ds(sh_width, sh_width)], preferred_element_type=f32)
        hidden = (jax.nn.silu(g) * u).astype(bf16)
        gp_load.start()
        sd_load.wait()
        for q in range(tp):
            cols = pl.ds(q * dq, dq)
            piece = jnp.dot(hidden, sd[:, cols], preferred_element_type=f32)
            st[:, :, cols] = piece.reshape(tp, each, dq)
        for k in range(ys):
            pair(st, e_half, ed_s, ed_r, k).start()

    def gate_step():
        gp_load.wait()

        def columns(j, _):
            cols = pl.ds(pl.multiple_of(j * bw, bw), bw)
            piece = jnp.dot(normed[...], w1[:, cols], preferred_element_type=f32)
            gate[:, cols] = jax.nn.gelu(piece)
            return 0

        lax.fori_loop(0, width // bw, columns, 0)
        for one in op_loads:
            one.start()

    def convolve():
        halo_copy().wait()
        ext[pl.ds(0, halo_rows), :] = jnp.where(me == 0, 0.0, halo[...].astype(f32))
        taps = taps_ref.shape[0]
        base = halo_rows - (taps - 1)
        first = (lax.broadcasted_iota(jnp.int32, (rows, bw), 0) == 0) & (me == 0)
        for b in range(blocks):
            cols = pl.ds(b * bw, bw)
            acc = taps_ref[0:1, cols] * ext[pl.ds(base, rows), cols]
            for k in range(1, taps):
                acc = acc + taps_ref[k : k + 1, cols] * ext[pl.ds(base + k, rows), cols]
            conv = acc.astype(bf16)
            ig = jax.nn.sigmoid(jnp.dot(conv, ig_ref[b], preferred_element_type=f32))
            dg = jax.nn.sigmoid(jnp.dot(conv, dg_ref[b], preferred_element_type=f32))
            ld = -lru_power * dg * soft_ref[0:1, cols]
            scale = jnp.where(first, 1.0, jnp.sqrt(-expm1_neg(2.0 * ld)))
            a_buf[:, cols] = jnp.exp(ld)
            b_buf[:, cols] = scale * ig * conv.astype(f32)

    def scan():
        row = lax.broadcasted_iota(jnp.int32, (8, width), 0)

        def block(r, carry):
            pc, sc = carry
            at = pl.ds(pl.multiple_of(r * 8, 8), 8)
            a, b = a_buf[at, :], b_buf[at, :]
            for sh in (1, 2, 4):
                keep = row >= sh
                b = jnp.where(keep, b + a * pltpu.roll(b, sh, 0), b)
                a = jnp.where(keep, a * pltpu.roll(a, sh, 0), a)
            b = b + a * sc
            a = a * pc
            a_buf[at, :] = a
            b_buf[at, :] = b
            return a[7:8, :], b[7:8, :]

        pl_last, s_last = lax.fori_loop(
            0, rows // 8, block, (jnp.ones((1, width), f32), jnp.zeros((1, width), f32))
        )
        ends[...] = jnp.where(row == 0, pl_last, s_last)
        for i in range(1, ep):
            end_copy(i).start()

    def carry_in():
        for i in range(1, ep):
            end_copy(i).wait()
        carry = jnp.zeros((1, width), f32)
        for i in range(ep - 1, 0, -1):
            carry = jnp.where(me >= i, got[i, 0:1, :] * carry + got[i, 1:2, :], carry)

        def finish(r, _):
            at = pl.ds(pl.multiple_of(r * 16, 16), 16)
            gated[at, :] = (gate[at, :] * (b_buf[at, :] + a_buf[at, :] * carry)).astype(bf16)
            return 0

        lax.fori_loop(0, rows // 16, finish, 0)

    def project_out():
        for one in op_loads:
            one.wait()
        for q in range(tp):
            piece = jnp.dot(
                gated[...], w1[pl.ds(q * width, width), :], preferred_element_type=f32
            )
            mt[:, :, pl.ds(q * dq, dq)] = piece.reshape(tp, each, dq)
        for k in range(ys):
            pair(mt, m_half, md_s, md_r, k).start()

    def shared_half():
        for k in range(1, ys):
            pair(st, e_half, ed_s, ed_r, k).wait_recv()
            e_out[k] = (e_half[k] + st[up(k)]).astype(bf16)
            ey_copy(k).start()

    def mixer_half():
        for k in range(1, ys):
            pair(mt, m_half, md_s, md_r, k).wait_recv()
            m_out[k] = (m_half[k] + mt[up(k)]).astype(bf16)
            my_copy(k).start()

    work = {
        0: project, 1: shared, 2: gate_step, 3: convolve, 4: scan, 5: carry_in, 6: project_out,
        ep - 1: shared_half, ep + 2: mixer_half,
    }

    def step(n, _):
        @pl.when((n > 0) & (n < ep))
        def _():
            i = n
            z_copy(i).wait_recv()
            for k in range(1, ys):
                y_copy(k, i).start()
            c_copy(0, i).start()

        @pl.when((n >= 2) & (n < ep + 1))
        def _():
            i = n - 1
            for k in range(1, ys):
                y_copy(k, i).wait_recv()
                c_copy(k, i).start()

        @pl.when(n == 2)
        def _():
            eg_load.wait()
            eu_load.wait()

        @pl.when((n >= 2) & (n < ep + 2))
        def _():
            i = n - 2

            @pl.when(i > 0)
            def _():
                for k in range(ys):
                    c_copy(k, i).wait_recv()

            gate_sum = up_sum = None
            for q in range(tp):
                x = recv[q, i]
                span = pl.ds(q * dq, dq)
                g = jnp.dot(x, eg[span, :], preferred_element_type=f32)
                u = jnp.dot(x, eu[span, :], preferred_element_type=f32)
                gate_sum = g if gate_sum is None else gate_sum + g
                up_sum = u if up_sum is None else up_sum + u
            hid[t, i] = (jax.nn.silu(gate_sum) * up_sum).astype(bf16)
            for k in range(1, ys):
                hy_copy(k, i).start()
            hc_copy(0, i).start()

        @pl.when((n >= 3) & (n < ep + 3))
        def _():
            i = n - 3
            for k in range(1, ys):
                hy_copy(k, i).wait_recv()
                hc_copy(k, i).start()

        @pl.when(n == 4)
        def _():
            wd_load.wait()
            for i in range(1, tp):
                w_copy(i).wait()

        @pl.when(n >= 4)
        def _():
            i = n - 4
            for k in range(ys):
                hc_copy(k, i).wait_recv()
            out = jnp.dot(hid[0, i], wd[0], preferred_element_type=f32)
            for q in range(1, tp):
                out = out + jnp.dot(hid[q, i], wd[q], preferred_element_type=f32)

            @pl.when(i == 0)
            def _():
                back[0] = out.astype(bf16)

            @pl.when(i > 0)
            def _():
                ret[i] = out.astype(bf16)
                b_copy(i).start()

        for at, task in work.items():
            pl.when(n == at)(task)
        return 0

    lax.fori_loop(0, ep + 4, step, 0)

    pair(mt, m_half, md_s, md_r, 0).wait_recv()
    whole = m_half[0] + mt[t]
    for k in range(1, ys):
        my_copy(k).wait_recv()
        whole = whole + m_in[k].astype(f32)
    mo_ref[...] = rms_scale(whole, ms_ref[...]).astype(bf16)
    pair(st, e_half, ed_s, ed_r, 0).wait_recv()
    whole = e_half[0] + st[t]
    for k in range(1, ys):
        ey_copy(k).wait_recv()
        whole = whole + e_in[k].astype(f32)
    total[...] = whole

    def arrive(i, _):
        b_copy(i).wait()
        return 0

    lax.fori_loop(1, ep, arrive, 0)
    flat = back[...].reshape(-1, dq)
    spot = lax.broadcasted_iota(jnp.int32, (rows, ep * cap), 1)
    routed = None
    for k in range(top):
        pick = (slots[:, k : k + 1] == spot).astype(f32).astype(bf16)
        term = weights[:, k : k + 1] * jnp.dot(pick, flat, preferred_element_type=f32)
        routed = term if routed is None else routed + term
    routed = routed.reshape(tp, each, dq)
    r_out[...] = routed.astype(bf16)
    for k in range(1, ys):
        for core in range(2):
            r_copy(k, core).start()
    r_buf[...] = routed
    r_copy(0, 1).start()
    total[:, mine] = total[:, mine] + r_buf[t]
    r_copy(0, 1).wait()
    near = pl.ds(pl.multiple_of(mate * dq, dq), dq)
    total[:, near] = total[:, near] + r_near[...]
    for k in range(1, ys):
        for core in range(2):
            r_copy(k, core).wait()
            q = down_of(k, lax.rem(c + core, 2))
            cols = pl.ds(pl.multiple_of(q * dq, dq), dq)
            total[:, cols] = total[:, cols] + r_in[q].astype(f32)
    eo_ref[...] = rms_scale(total[...], es_ref[...]).astype(bf16)

    def settle(i, _):
        for k in range(1, ys):
            hy_copy(k, i).wait_send()
        for k in range(ys):
            hc_copy(k, i).wait_send()

        @pl.when(i > 0)
        def _():
            for k in range(1, ys):
                y_copy(k, i).wait_send()
            for k in range(ys):
                c_copy(k, i).wait_send()
            z_copy(i).wait_send()

        return 0

    lax.fori_loop(0, ep, settle, 0)
    for k in range(ys):
        pair(mt, m_half, md_s, md_r, k).wait_send()
        pair(st, e_half, ed_s, ed_r, k).wait_send()
    for k in range(1, ys):
        my_copy(k).wait_send()
        ey_copy(k).wait_send()


def dma(*shape):
    return pltpu.SemaphoreType.DMA(shape)


def layer(ep, tp, small, large):
    rows, depth = large[0].shape
    width = large[2].shape[1]
    hf, hs = large[5].shape[1], large[8].shape[1]
    top = small[0].shape[1]
    each, ys, dq = rows // tp, tp // 2, depth // tp
    cap = rows * top * 3 // (2 * ep)
    V = pltpu.VMEM
    return pl.pallas_call(
        functools.partial(layer_kernel, ep, tp, top),
        out_shape=[jax.ShapeDtypeStruct((each, depth), bf16)] * 2,
        in_specs=[pl.BlockSpec(memory_space=V)] * len(small)
        + [pl.BlockSpec(memory_space=pl.ANY)] * len(large),
        out_specs=[pl.BlockSpec(memory_space=V)] * 2,
        scratch_shapes=[
            V((ep, cap, dq), bf16),
            V((rows, depth), bf16),
            V((rows, depth), bf16),
            V((ys, each, depth), bf16),
            V((tp, each, dq), bf16),
            V((each, dq), f32),
            V((depth, width), bf16),
            V((depth, hf), bf16),
            V((depth, hf), bf16),
            V((tp, hf, dq), bf16),
            V((hs, depth), bf16),
            V((tp, ep, cap, dq), bf16),
            V((tp, ep, cap, hf), bf16),
            V((ep, cap, dq), bf16),
            V((ep, cap, dq), bf16),
            V((tp, each, depth), f32),
            V((tp, each, depth), f32),
            V((ys, each, depth), f32),
            V((ys, each, depth), f32),
            V((ys, each, depth), bf16),
            V((ys, each, depth), bf16),
            V((ys, each, depth), bf16),
            V((tp, each, dq), f32),
            V((tp, each, dq), bf16),
            V((each, depth), f32),
            V((rows, width), f32),
            V((rows, width), f32),
            V((rows, width), f32),
            V((halo_rows + rows, width), f32),
            V((halo_rows, width), bf16),
            V((halo_rows, width), bf16),
            V((8, width), f32),
            V((ep, 8, width), f32),
            V((rows, width), bf16),
            dma(10 + tp), pltpu.SemaphoreType.DMA, pltpu.SemaphoreType.DMA, dma(ep), dma(ep),
            dma(ep), dma(ep),
            dma(ys, ep), dma(ys, ep),
            dma(ys, ep), dma(ys, ep),
            dma(ys, ep), dma(ys, ep),
            dma(ys, ep), dma(ys, ep),
            dma(tp), dma(tp),
            dma(ep), dma(ep),
            dma(ys), dma(ys), dma(ys), dma(ys),
            dma(ys), dma(ys), dma(ys), dma(ys),
            dma(tp), dma(tp),
        ],
        compiler_params=pltpu.CompilerParams(
            collective_id=0, has_side_effects=True, vmem_limit_bytes=67000000
        ),
        name="layer",
    )(*small, *large)


def body(
    mixer_rows, mixer_gain, gate_proj, input_proj, conv_taps, input_gates, decay_gates,
    decay_offset, out_proj, mixer_scale, expert_rows, expert_gain, route_ids, route_weights,
    expert_gate, expert_up, expert_down, shared_gate, shared_up, shared_down, expert_scale,
):
    ep, tp = lax.axis_size("ep"), lax.axis_size("tp")
    me = lax.axis_index("ep")
    tokens = expert_rows.shape[0]
    top = route_ids.shape[1]
    cap = tokens * top * 3 // (2 * ep)
    offset_ids = lax.rem(route_ids + (ep - me), ep)
    indicator = jnp.sum(
        (offset_ids[:, :, None] == jnp.arange(ep, dtype=jnp.int32)).astype(f32), axis=1
    )
    below = (
        jnp.arange(tokens)[:, None] > jnp.arange(tokens)[None, :]
    ).astype(bf16)
    earlier = jnp.dot(below, indicator.astype(bf16), preferred_element_type=f32)
    chosen = (offset_ids[:, :, None] == jnp.arange(ep, dtype=jnp.int32)).astype(f32)
    position = jnp.sum(chosen * earlier[:, None, :], axis=2).astype(jnp.int32)
    slot_ids = offset_ids * cap + position
    soft = jax.nn.softplus(-decay_offset).reshape(1, -1)
    gains = [x.reshape(1, -1) for x in (mixer_gain, expert_gain, mixer_scale, expert_scale)]
    small = (
        slot_ids, slot_ids.T, conv_taps, input_gates, decay_gates, soft, route_weights, *gains,
    )
    large = (
        mixer_rows, expert_rows, input_proj, gate_proj, out_proj, expert_gate[0], expert_up[0], expert_down[0],
        shared_gate, shared_up, shared_down,
    )
    return tuple(layer(ep, tp, small, large))


def solution(mesh):
    placed = (
        P("ep", None),
        P(),
        P(None, "tp"),
        P(None, "tp"),
        P(None, "tp"),
        P("tp", None, None),
        P("tp", None, None),
        P("tp"),
        P("tp", None),
        P(),
        P("ep", None),
        P(),
        P("ep", None),
        P("ep", None),
        P("ep", None, "tp"),
        P("ep", None, "tp"),
        P("ep", "tp", None),
        P(None, "tp"),
        P(None, "tp"),
        P("tp", None),
        P(),
    )
    return jax.shard_map(
        body,
        mesh=mesh,
        in_specs=placed,
        out_specs=(P(("ep", "tp"), None), P(("ep", "tp"), None)),
        check_vma=False,
    )
```

profile of v0, /device:TPU:1, one launch (start us, length us, event | category | flops | bytes accessed | tf_op | source)
XLA Modules:
  0.0 118.3 jit_solution(1110523707174051068)
XLA Ops:
  0.6 0.7 compare_select_fusion.1
  1.3 0.2 fusion
  1.5 0.7 convert_add_fusion
  2.2 0.0 copy-start
  2.2 1.3 %compare_select_fusion = f32[1024]{0:T(1024)} fusion(f32[1024]{0:T(1024)} %param.28), kind=kLoop, calls=%fused_computation.5 | loop fusion | flops 7168 | bytes 8192 | tf_op jit(solution)/shard_map/jit(softplus)/select_n | solution.py:563
  3.5 0.8 copy.27.slots
  4.3 1.5 %copy.28.weights = f32[256,2]{1,0:T(8,128)} copy(f32[256,2]{0,1:T(2,128)} %param.34) | data formatting | bytes 4096 | tf_op args[13]
  5.8 0.0 copy-done
  5.8 108.7 %layer.1 = (bf16[64,4096]{1,0:T(8,128)(2,1)}, bf16[64,4096]{1,0:T(8,128)(2,1)}) custom-call(s32[256,2]{1,0:T(8,128)} %copy.27.slots, s32[2,256]{1,0:T(2,128)} %bitcast.13, f32[4,1024]{1,0:T(4,128)} %taps_ref.1, bf16[4,256,256]{2,1,0:T(8,128)(2,1)} %ig_ref.1, bf16[4,256,256]{2,1,0:T(8,128)(2,1)} %dg_ref.1, f32[1,1024]{1,0:T(1,128)} %bitcast.18, ...), custom_call_target="tpu_custom_call" | custom-call | tf_op jit(solution)/shard_map/layer/pallas_call | solution.py:482
  114.5 1.9 %copy.31 = bf16[64,4096]{1,0:T(8,128)(2,1)} copy(bf16[64,4096]{1,0:T(8,128)(2,1)} %get-tuple-element.4) | data formatting | bytes 1048576
  116.4 1.9 %copy.32 = bf16[64,4096]{1,0:T(8,128)(2,1)} copy(bf16[64,4096]{1,0:T(8,128)(2,1)} %get-tuple-element.5) | data formatting | bytes 1048576
  (2 shorter events, 0.1 us)
Async XLA Ops:
  2.2 3.6 %copy-start = (s32[256,2]{0,1:T(2,128)}, s32[256,2]{0,1:T(2,128)S(1)}, u32[]{:S(2)}) copy-start(s32[256,2]{0,1:T(2,128)S(1)} %convert_add_fusion) | copy-start | bytes 6148
where the time goes:
time: 119 us; the launch traced here: 118 us
  Pallas kernels  109 us (92%)
  local copies, waits for them, and re-layouts  6.01 us (5%)
  other arithmetic  2.74 us (2%)
    pallas_call x1, Pallas kernels, layer(): pl.pallas_call(functools.partial(layer_kernel, ep, tp, top), out_shape=[j...  109 us
    unnamed x5, local copies, waits for them, and re-layouts  5.21 us

commit v1 on v0

v1 whole, which is shorter than its diff:
```python
import functools

import jax
import jax.numpy as jnp
from jax import lax
from jax.experimental import pallas as pl
from jax.experimental.pallas import tpu as pltpu
from jax.sharding import PartitionSpec as P

eps = 1e-06
lru_power = 8.0
halo_rows = 16
MESH = pl.DeviceIdType.MESH
f32 = jnp.float32
bf16 = jnp.bfloat16


def rms_scale(values, scale):
    floats = values.astype(f32)
    return floats * lax.rsqrt(jnp.mean(floats * floats, axis=-1, keepdims=True) + eps) * scale


def remote(src, dst, send_sem, recv_sem, ep_at, tp_at):
    return pltpu.make_async_remote_copy(
        src_ref=src,
        dst_ref=dst,
        send_sem=send_sem,
        recv_sem=recv_sem,
        device_id=(ep_at, tp_at),
        device_id_type=MESH,
    )


def greet(peers):
    barrier = pltpu.get_barrier_semaphore()
    for ep_at, tp_at in peers:
        pl.semaphore_signal(barrier, inc=1, device_id=(ep_at, tp_at), device_id_type=MESH)
    pl.semaphore_wait(barrier, len(peers))


def expm1_neg(y):
    series = y * (1 + y / 2 * (1 + y / 3 * (1 + y / 4 * (1 + y / 5 * (1 + y / 6 * (1 + y / 7))))))
    return jnp.where(y > -0.35, series, jnp.exp(y) - 1.0)


def softplus_neg(x):
    u = jnp.exp(-jnp.abs(x))
    series = u * (1 - u * (1 / 2 - u * (1 / 3 - u * (1 / 4 - u * (1 / 5 - u / 6)))))
    return jnp.maximum(-x, 0.0) + jnp.where(u < 0.05, series, jnp.log(1.0 + u))


def layer_kernel(
    ep, tp, top,
    ids_ref, weights_ref, taps_ref, ig_ref, dg_ref, offset_ref, mg_ref, xg_ref, ms_ref, es_ref,
    rows_hbm, tokens_hbm, ip_hbm, gp_hbm, op_hbm, eg_hbm, eu_hbm, ed, sg_hbm, su_hbm, sd_hbm,
    mo_ref, eo_ref,
    outq, normed, en, e_out, r_out, r_near,
    w1, eg, eu, wd, sd, recv, hid, ret, back, mt, st, m_half, e_half, m_out, m_in, e_in,
    r_buf, r_in, total, gate, a_buf, b_buf, ext, ends, got, gated, meta, cols_ref,
    load_sem, halo_send, halo_recv, end_send, end_recv,
    z_s, z_r, y_s, y_r, c_s, c_r, hy_s, hy_r, hc_s, hc_r, w_s, w_r, b_s, b_r,
    md_s, md_r, ed_s, ed_r, my_s, my_r, ey_s, ey_r, r_s, r_r,
):
    me, t = lax.axis_index("ep"), lax.axis_index("tp")
    ys = tp // 2
    y, c = t // 2, lax.rem(t, 2)
    mate = y * 2 + 1 - c
    dq = outq.shape[3]
    cap = outq.shape[2]
    rows, width = ext.shape[0] - halo_rows, ext.shape[1]
    each = rows // tp
    blocks, bw = ig_ref.shape[0], ig_ref.shape[1]
    sh_width = sd.shape[0]
    half, quarter = ep // 2, ep // 4
    groups = ep // 2
    inner = lax.rem(me // quarter + 1, 4) // 2

    def at_y(k):
        return lax.rem(y + k, ys)

    def up(k):
        return at_y(k) * 2 + c

    def down_of(k, core):
        return lax.rem(y + ys - k, ys) * 2 + core

    def partner(i):
        out, bit = 0, 1
        while bit < ep:
            out = out + lax.rem(me // bit + i // bit, 2) * bit
            bit *= 2
        return out

    def far(j):
        return half + lax.rem(j + inner * quarter, half)

    def base_of(g):
        return 2 * g if 2 * g < half else far(2 * g - half)

    def blocks_of(g):
        base = base_of(g)
        return [i for i in (base, base + 1) if not (isinstance(i, int) and i == 0)]

    def load(src, dst, at):
        return pltpu.make_async_copy(src, dst, load_sem.at[at])

    tokens_load, rows_load = load(tokens_hbm, en, 0), load(
        rows_hbm, normed.at[pl.ds(halo_rows, rows)], 9 + tp
    )
    tokens_load.start()
    rows_load.start()
    ip_load = load(ip_hbm, w1, 1)
    ip_load.start()

    greet(
        [(lax.rem(me + i, ep), t) for i in range(1, ep)]
        + [(me, lax.rem(t + i, tp)) for i in range(1, tp)]
    )

    def z_copy(i, yy):
        return remote(
            outq.at[yy, i], recv.at[yy * 2 + c, i], z_s.at[yy, i], z_r.at[yy, i], partner(i), t
        )

    def y_copy(k, i):
        return remote(recv.at[t, i], recv.at[t, i], y_s.at[k, i], y_r.at[k, i], me, up(k))

    def c_copy(k, i):
        q = down_of(k, c)
        return remote(recv.at[q, i], recv.at[q, i], c_s.at[k, i], c_r.at[k, i], me, mate)

    def hy_copy(k, g):
        part = hid.at[t, pl.ds(base_of(g), 2)]
        return remote(part, part, hy_s.at[k, g], hy_r.at[k, g], me, up(k))

    def hc_copy(k, g):
        part = hid.at[down_of(k, c), pl.ds(base_of(g), 2)]
        return remote(part, part, hc_s.at[k, g], hc_r.at[k, g], me, mate)

    def w_copy(i):
        q = lax.rem(t + i, tp)
        return remote(
            ed.at[:, pl.ds(pl.multiple_of(q * dq, dq), dq)], wd.at[t],
            w_s.at[i], w_r.at[i], me, q,
        )

    def b_copy(i):
        return remote(ret.at[i], back.at[i], b_s.at[i], b_r.at[i], partner(i), t)

    def halo_copy():
        return remote(
            rows_hbm.at[pl.ds(rows - halo_rows, halo_rows)], normed.at[pl.ds(0, halo_rows)],
            halo_send, halo_recv, lax.rem(me + 1, ep), t,
        )

    def end_copy(i):
        return remote(ends, got.at[i], end_send.at[i], end_recv.at[i], lax.rem(me + i, ep), t)

    def pair(ref, half, s, r, k):
        return remote(ref.at[at_y(k) * 2 + 1 - c], half.at[k], s.at[k], r.at[k], me, mate)

    def my_copy(k):
        return remote(m_out.at[k], m_in.at[k], my_s.at[k], my_r.at[k], me, up(k))

    def ey_copy(k):
        return remote(e_out.at[k], e_in.at[k], ey_s.at[k], ey_r.at[k], me, up(k))

    def r_copy(k, core):
        j, q = 2 * k + core, at_y(k) * 2 + lax.rem(c + core, 2)
        if k == 0:
            return remote(r_buf.at[q], r_near, r_s.at[j], r_r.at[j], me, q)
        return remote(r_out.at[q], r_in.at[t], r_s.at[j], r_r.at[j], me, q)

    def normalize(ref, gain):
        def some(r, _):
            at = pl.ds(pl.multiple_of(r * 16, 16), 16)
            ref[at, :] = rms_scale(ref[at, :], gain[...]).astype(bf16)
            return 0

        lax.fori_loop(0, ref.shape[0] // 16, some, 0)

    halo_copy().start()
    member = lax.broadcasted_iota(jnp.int32, (ep, rows), 0)
    chosen = [
        (jnp.bitwise_xor(ids_ref[k : k + 1, :], me) == member).astype(f32) for k in range(top)
    ]
    named = chosen[0]
    for k in range(1, top):
        named = named + chosen[k]
    before = lax.broadcasted_iota(jnp.int32, (rows, rows), 0) < lax.broadcasted_iota(
        jnp.int32, (rows, rows), 1
    )
    earlier = jnp.dot(
        named.astype(bf16), before.astype(f32).astype(bf16), preferred_element_type=f32
    )
    spots = earlier + member.astype(f32) * cap
    meta[...] = jnp.zeros_like(meta)
    for k in range(top):
        meta[k : k + 1, :] = jnp.sum(chosen[k] * spots, axis=0, keepdims=True)
        meta[top + k : top + k + 1, :] = weights_ref[k : k + 1, :]
    cols_ref[...] = meta[...].T

    tokens_load.wait()
    for i in range(1, tp):
        w_copy(i).start()
    eg_load, eu_load = load(eg_hbm, eg, 2), load(eu_hbm, eu, 3)
    eg_load.start()
    eu_load.start()
    wd_load = load(ed.at[:, pl.ds(pl.multiple_of(t * dq, dq), dq)], wd.at[t], 4)
    wd_load.start()
    sd_load = load(sd_hbm, sd, 5)
    sd_load.start()
    normalize(en, xg_ref)
    mine = pl.ds(pl.multiple_of(t * dq, dq), dq)

    def place(i):
        spot = (lax.broadcasted_iota(jnp.int32, (cap, rows), 0) + i * cap).astype(f32)
        hot = meta[0:1, :] == spot
        for k in range(1, top):
            hot = hot | (meta[k : k + 1, :] == spot)
        return hot.astype(f32).astype(bf16)

    def dispatch_near(i, _):
        hot = place(i)
        for yy in range(ys):
            part = pl.ds(pl.multiple_of((yy * 2 + c) * dq, dq), dq)
            outq[yy, i] = jnp.dot(hot, en[:, part], preferred_element_type=f32).astype(bf16)
            z_copy(i, yy).start()
        return 0

    def dispatch_far(j, _):
        i = far(j)
        outq[y, i] = jnp.dot(place(i), en[:, mine], preferred_element_type=f32).astype(bf16)
        z_copy(i, y).start()
        return 0

    def dispatch_fars(when, lo, hi):
        @pl.when(inner == when)
        def _():
            lax.fori_loop(lo, hi, dispatch_far, 0)

    lax.fori_loop(1, 2, dispatch_near, 0)
    dispatch_fars(1, 0, quarter + 1)
    lax.fori_loop(2, half - 1, dispatch_near, 0)
    local = place(0)
    for q in range(tp):
        recv[q, 0] = jnp.dot(
            local, en[:, pl.ds(q * dq, dq)], preferred_element_type=f32
        ).astype(bf16)
    rows_load.wait()
    halo_copy().wait_recv()
    normalize(normed, mg_ref)
    sg_load = load(sg_hbm, w1.at[:, pl.ds(0, sh_width)], 6)
    su_load = load(su_hbm, w1.at[:, pl.ds(sh_width, sh_width)], 7)
    gp_load = load(gp_hbm, w1, 8)
    op_loads = [
        load(op_hbm.at[:, pl.ds(q * dq, dq)], w1.at[pl.ds(q * width, width), :], 9 + q)
        for q in range(tp)
    ]

    def project():
        ip_load.wait()

        def columns(j, _):
            cols = pl.ds(pl.multiple_of(j * bw, bw), bw)
            piece = jnp.dot(normed[...], w1[:, cols], preferred_element_type=f32)
            ext[:, cols] = piece.astype(bf16).astype(f32)
            return 0

        lax.fori_loop(0, width // bw, columns, 0)
        gp_load.start()

        @pl.when(me == 0)
        def _():
            ext[pl.ds(0, halo_rows), :] = jnp.zeros((halo_rows, width), f32)

    def shared():
        sg_load.wait()
        su_load.wait()
        g = jnp.dot(en[...], w1[:, pl.ds(0, sh_width)], preferred_element_type=f32)
        u = jnp.dot(en[...], w1[:, pl.ds(sh_width, sh_width)], preferred_element_type=f32)
        hidden = (jax.nn.silu(g) * u).astype(bf16)
        for one in op_loads:
            one.start()
        sd_load.wait()
        for q in range(tp):
            cols = pl.ds(q * dq, dq)
            piece = jnp.dot(hidden, sd[:, cols], preferred_element_type=f32)
            st[:, :, cols] = piece.reshape(tp, each, dq)
        for k in range(ys):
            pair(st, e_half, ed_s, ed_r, k).start()

    def gate_step():
        gp_load.wait()

        def columns(j, _):
            cols = pl.ds(pl.multiple_of(j * bw, bw), bw)
            piece = jnp.dot(
                normed[pl.ds(halo_rows, rows)], w1[:, cols], preferred_element_type=f32
            )
            gate[:, cols] = jax.nn.gelu(piece)
            return 0

        lax.fori_loop(0, width // bw, columns, 0)
        sg_load.start()
        su_load.start()

    def convolve():
        taps = taps_ref.shape[0]
        base = halo_rows - (taps - 1)
        first = (lax.broadcasted_iota(jnp.int32, (rows, bw), 0) == 0) & (me == 0)
        for b in range(blocks):
            cols = pl.ds(b * bw, bw)
            acc = taps_ref[0:1, cols] * ext[pl.ds(base, rows), cols]
            for k in range(1, taps):
                acc = acc + taps_ref[k : k + 1, cols] * ext[pl.ds(base + k, rows), cols]
            conv = acc.astype(bf16)
            ig = jax.nn.sigmoid(jnp.dot(conv, ig_ref[b], preferred_element_type=f32))
            dg = jax.nn.sigmoid(jnp.dot(conv, dg_ref[b], preferred_element_type=f32))
            ld = -lru_power * dg * softplus_neg(offset_ref[0:1, cols])
            scale = jnp.where(first, 1.0, jnp.sqrt(-expm1_neg(2.0 * ld)))
            a_buf[:, cols] = jnp.exp(ld)
            b_buf[:, cols] = scale * ig * conv.astype(f32)

    def scan():
        row = lax.broadcasted_iota(jnp.int32, (8, width), 0)

        def block(r, carry):
            pc, sc = carry
            at = pl.ds(pl.multiple_of(r * 8, 8), 8)
            a, b = a_buf[at, :], b_buf[at, :]
            for sh in (1, 2, 4):
                keep = row >= sh
                b = jnp.where(keep, b + a * pltpu.roll(b, sh, 0), b)
                a = jnp.where(keep, a * pltpu.roll(a, sh, 0), a)
            b = b + a * sc
            a = a * pc
            a_buf[at, :] = a
            b_buf[at, :] = b
            return a[7:8, :], b[7:8, :]

        pl_last, s_last = lax.fori_loop(
            0, rows // 8, block, (jnp.ones((1, width), f32), jnp.zeros((1, width), f32))
        )
        ends[...] = jnp.where(row == 0, pl_last, s_last)
        for i in range(1, ep):
            end_copy(i).start()

    def carry_in():
        for i in range(1, ep):
            end_copy(i).wait()
        carry = jnp.zeros((1, width), f32)
        for i in range(ep - 1, 0, -1):
            carry = jnp.where(me >= i, got[i, 0:1, :] * carry + got[i, 1:2, :], carry)

        def finish(r, _):
            at = pl.ds(pl.multiple_of(r * 16, 16), 16)
            gated[at, :] = (gate[at, :] * (b_buf[at, :] + a_buf[at, :] * carry)).astype(bf16)
            return 0

        lax.fori_loop(0, rows // 16, finish, 0)

    def project_out():
        for one in op_loads:
            one.wait()
        for q in range(tp):
            piece = jnp.dot(
                gated[...], w1[pl.ds(q * width, width), :], preferred_element_type=f32
            )
            mt[:, :, pl.ds(q * dq, dq)] = piece.reshape(tp, each, dq)
        for k in range(ys):
            pair(mt, m_half, md_s, md_r, k).start()

    def shared_half():
        for k in range(1, ys):
            pair(st, e_half, ed_s, ed_r, k).wait_recv()
            e_out[k] = (e_half[k] + st[up(k)]).astype(bf16)
            ey_copy(k).start()

    def mixer_half():
        for k in range(1, ys):
            pair(mt, m_half, md_s, md_r, k).wait_recv()
            m_out[k] = (m_half[k] + mt[up(k)]).astype(bf16)
            my_copy(k).start()

    def arrive(g):
        for i in blocks_of(g):
            if 2 * g < half:
                for yy in range(ys):
                    z_copy(i, yy).wait_recv()
                for k in range(ys):
                    c_copy(k, i).start()
            else:
                z_copy(i, y).wait_recv()
                for k in range(1, ys):
                    y_copy(k, i).start()
                c_copy(0, i).start()

    def forward(g):
        if 2 * g >= half:
            for i in blocks_of(g):
                for k in range(1, ys):
                    y_copy(k, i).wait_recv()
                    c_copy(k, i).start()

    def feed(g):
        for i in blocks_of(g):
            for k in range(ys):
                c_copy(k, i).wait_recv()
        both = pl.ds(base_of(g), 2)
        gate_sum = up_sum = None
        for q in range(tp):
            x = recv[q, both].reshape(2 * cap, dq)
            span = pl.ds(q * dq, dq)
            g_part = jnp.dot(x, eg[span, :], preferred_element_type=f32)
            u_part = jnp.dot(x, eu[span, :], preferred_element_type=f32)
            gate_sum = g_part if gate_sum is None else gate_sum + g_part
            up_sum = u_part if up_sum is None else up_sum + u_part
        hidden = (jax.nn.silu(gate_sum) * up_sum).astype(bf16)
        hid[t, both] = hidden.reshape(2, cap, hidden.shape[1])
        for k in range(1, ys):
            hy_copy(k, g).start()
        hc_copy(0, g).start()

    def pass_on(g):
        for k in range(1, ys):
            hy_copy(k, g).wait_recv()
            hc_copy(k, g).start()

    def finish(g):
        for k in range(ys):
            hc_copy(k, g).wait_recv()
        both = pl.ds(base_of(g), 2)
        out = None
        for q in range(tp):
            h = hid[q, both].reshape(2 * cap, hid.shape[3])
            part = jnp.dot(h, wd[q], preferred_element_type=f32)
            out = part if out is None else out + part
        out = out.astype(bf16).reshape(2, cap, dq)
        if g == 0:
            back[0] = out[0]
        ret[both] = out
        for i in blocks_of(g):
            b_copy(i).start()

    first_far = groups // 2
    project()
    convolve()
    scan()
    lax.fori_loop(half - 1, half, dispatch_near, 0)
    dispatch_fars(1, quarter + 1, half)
    dispatch_fars(0, 0, half)
    gate_step()
    eg_load.wait()
    eu_load.wait()
    arrive(0)
    arrive(first_far)
    feed(0)
    shared()
    for g in range(1, first_far):
        arrive(g)
        feed(g)
    carry_in()
    project_out()
    wd_load.wait()
    for i in range(1, tp):
        w_copy(i).wait()
    forward(first_far)
    feed(first_far)
    pass_on(0)
    finish(0)
    for g in range(first_far + 1, groups):
        arrive(g)
        pass_on(g - 1)
        finish(g - 1)
        if g == first_far + 1:
            for near in range(1, first_far):
                pass_on(near)
                finish(near)
        forward(g)
        feed(g)
    shared_half()
    mixer_half()
    pass_on(groups - 1)
    finish(groups - 1)

    def combine(lo, count):
        flat = back[pl.ds(lo, count)].reshape(count * cap, dq)
        spot = (lax.broadcasted_iota(jnp.int32, (rows, count * cap), 1) + lo * cap).astype(f32)
        out = None
        for k in range(top):
            pick = (cols_ref[:, k : k + 1] == spot).astype(f32).astype(bf16)
            term = cols_ref[:, top + k : top + k + 1] * jnp.dot(
                pick, flat, preferred_element_type=f32
            )
            out = term if out is None else out + term
        return out.reshape(tp, each, dq)

    for i in range(1, half):
        b_copy(i).wait_recv()
    r_buf[...] = combine(0, half)
    pair(st, e_half, ed_s, ed_r, 0).wait_recv()
    whole = e_half[0] + st[t]
    for k in range(1, ys):
        ey_copy(k).wait_recv()
        whole = whole + e_in[k].astype(f32)
    total[...] = whole
    pair(mt, m_half, md_s, md_r, 0).wait_recv()
    whole = m_half[0] + mt[t]
    for k in range(1, ys):
        my_copy(k).wait_recv()
        whole = whole + m_in[k].astype(f32)
    mo_ref[...] = rms_scale(whole, ms_ref[...]).astype(bf16)
    for i in range(half, ep):
        b_copy(i).wait_recv()
    routed = r_buf[...] + combine(half, half)
    r_out[...] = routed.astype(bf16)
    for k in range(1, ys):
        for core in range(2):
            r_copy(k, core).start()
    r_buf[...] = routed
    r_copy(0, 1).start()
    total[:, mine] = total[:, mine] + r_buf[t]
    r_copy(0, 1).wait()
    near = pl.ds(pl.multiple_of(mate * dq, dq), dq)
    total[:, near] = total[:, near] + r_near[...]
    for k in range(1, ys):
        for core in range(2):
            r_copy(k, core).wait()
            q = down_of(k, lax.rem(c + core, 2))
            cols = pl.ds(pl.multiple_of(q * dq, dq), dq)
            total[:, cols] = total[:, cols] + r_in[q].astype(f32)
    eo_ref[...] = rms_scale(total[...], es_ref[...]).astype(bf16)

    def settle_near(i, _):
        for yy in range(ys):
            z_copy(i, yy).wait_send()
        for k in range(ys):
            c_copy(k, i).wait_send()
        b_copy(i).wait_send()
        return 0

    def settle_far(i, _):
        z_copy(i, y).wait_send()
        for k in range(1, ys):
            y_copy(k, i).wait_send()
        for k in range(ys):
            c_copy(k, i).wait_send()
        b_copy(i).wait_send()
        return 0

    halo_copy().wait_send()
    lax.fori_loop(1, half, settle_near, 0)
    lax.fori_loop(half, ep, settle_far, 0)
    for g in range(groups):
        for k in range(1, ys):
            hy_copy(k, g).wait_send()
        for k in range(ys):
            hc_copy(k, g).wait_send()
    for k in range(ys):
        pair(mt, m_half, md_s, md_r, k).wait_send()
        pair(st, e_half, ed_s, ed_r, k).wait_send()
    for k in range(1, ys):
        my_copy(k).wait_send()
        ey_copy(k).wait_send()


def dma(*shape):
    return pltpu.SemaphoreType.DMA(shape)


def layer(ep, tp, small, large):
    rows, depth = large[0].shape
    width = large[2].shape[1]
    hf, hs = large[5].shape[1], large[8].shape[1]
    top = small[0].shape[0]
    each, ys, dq = rows // tp, tp // 2, depth // tp
    cap = rows * top * 3 // (2 * ep)
    V = pltpu.VMEM
    return pl.pallas_call(
        functools.partial(layer_kernel, ep, tp, top),
        out_shape=[jax.ShapeDtypeStruct((each, depth), bf16)] * 2,
        in_specs=[pl.BlockSpec(memory_space=V)] * len(small)
        + [pl.BlockSpec(memory_space=pl.ANY)] * len(large),
        out_specs=[pl.BlockSpec(memory_space=V)] * 2,
        scratch_shapes=[
            V((ys, ep, cap, dq), bf16),
            V((halo_rows + rows, depth), bf16),
            V((rows, depth), bf16),
            V((ys, each, depth), bf16),
            V((tp, each, dq), bf16),
            V((each, dq), f32),
            V((depth, width), bf16),
            V((depth, hf), bf16),
            V((depth, hf), bf16),
            V((tp, hf, dq), bf16),
            V((hs, depth), bf16),
            V((tp, ep, cap, dq), bf16),
            V((tp, ep, cap, hf), bf16),
            V((ep, cap, dq), bf16),
            V((ep, cap, dq), bf16),
            V((tp, each, depth), f32),
            V((tp, each, depth), f32),
            V((ys, each, depth), f32),
            V((ys, each, depth), f32),
            V((ys, each, depth), bf16),
            V((ys, each, depth), bf16),
            V((ys, each, depth), bf16),
            V((tp, each, dq), f32),
            V((tp, each, dq), bf16),
            V((each, depth), f32),
            V((rows, width), f32),
            V((rows, width), f32),
            V((rows, width), f32),
            V((halo_rows + rows, width), f32),
            V((8, width), f32),
            V((ep, 8, width), f32),
            V((rows, width), bf16),
            V((128, rows), f32),
            V((rows, 128), f32),
            dma(10 + tp), pltpu.SemaphoreType.DMA, pltpu.SemaphoreType.DMA, dma(ep), dma(ep),
            dma(ys, ep), dma(ys, ep),
            dma(ys, ep), dma(ys, ep),
            dma(ys, ep), dma(ys, ep),
            dma(ys, ep // 2), dma(ys, ep // 2),
            dma(ys, ep // 2), dma(ys, ep // 2),
            dma(tp), dma(tp),
            dma(ep), dma(ep),
            dma(ys), dma(ys), dma(ys), dma(ys),
            dma(ys), dma(ys), dma(ys), dma(ys),
            dma(tp), dma(tp),
        ],
        compiler_params=pltpu.CompilerParams(
            collective_id=0, has_side_effects=True, vmem_limit_bytes=67000000
        ),
        name="layer",
    )(*small, *large)


def body(
    mixer_rows, mixer_gain, gate_proj, input_proj, conv_taps, input_gates, decay_gates,
    decay_offset, out_proj, mixer_scale, expert_rows, expert_gain, route_ids, route_weights,
    expert_gate, expert_up, expert_down, shared_gate, shared_up, shared_down, expert_scale,
):
    ep, tp = lax.axis_size("ep"), lax.axis_size("tp")
    gains = [x.reshape(1, -1) for x in (mixer_gain, expert_gain, mixer_scale, expert_scale)]
    small = (
        route_ids.T, route_weights.T, conv_taps, input_gates, decay_gates,
        decay_offset.reshape(1, -1), *gains,
    )
    large = (
        mixer_rows, expert_rows, input_proj, gate_proj, out_proj, expert_gate[0], expert_up[0], expert_down[0],
        shared_gate, shared_up, shared_down,
    )
    return tuple(layer(ep, tp, small, large))


def solution(mesh):
    placed = (
        P("ep", None),
        P(),
        P(None, "tp"),
        P(None, "tp"),
        P(None, "tp"),
        P("tp", None, None),
        P("tp", None, None),
        P("tp"),
        P("tp", None),
        P(),
        P("ep", None),
        P(),
        P("ep", None),
        P("ep", None),
        P("ep", None, "tp"),
        P("ep", None, "tp"),
        P("ep", "tp", None),
        P(None, "tp"),
        P(None, "tp"),
        P("tp", None),
        P(),
    )
    return jax.shard_map(
        body,
        mesh=mesh,
        in_specs=placed,
        out_specs=(P(("ep", "tp"), None), P(("ep", "tp"), None)),
        check_vma=False,
    )
```

time: 119 us -> 109 us (0.916)
  Pallas kernels: 109 us -> 105 us
  other arithmetic: 2.74 us -> 0 us
  local copies, waits for them, and re-layouts: 6.01 us -> 3.74 us
    pallas_call x1, Pallas kernels: 109 us -> 105 us  [layer(): pl.pallas_call(functools.partial(layer_kernel, ep, tp, top), out_shape=[j...]
    unnamed x5 -> x2, local copies, waits for them, and re-layouts: 5.21 us -> 3.74 us
    select_n x1 -> x0, other arithmetic: 1.3 us -> none  [body(): soft = jax.nn.softplus(-decay_offset).reshape(1, -1)]
where the time goes in v1:
time: 109 us
  Pallas kernels  105 us (96%)
  local copies, waits for them, and re-layouts  3.74 us (3%)
    pallas_call x1, Pallas kernels, layer(): pl.pallas_call(functools.partial(layer_kernel, ep, tp, top), out_shape=[j...  105 us
    unnamed x2, local copies, waits for them, and re-layouts  3.74 us

profile of v1, /device:TPU:1, one launch (start us, length us, event | category | flops | bytes accessed | tf_op | source)
XLA Modules:
  0.0 109.2 jit_solution(15021100819293478238)
XLA Ops:
  0.6 104.9 %layer.1 = (bf16[64,4096]{1,0:T(8,128)(2,1)}, bf16[64,4096]{1,0:T(8,128)(2,1)}) custom-call(s32[2,256]{1,0:T(2,128)} %bitcast.18, f32[2,256]{1,0:T(2,128)} %bitcast.19, f32[4,1024]{1,0:T(4,128)} %taps_ref.1, bf16[4,256,256]{2,1,0:T(8,128)(2,1)} %ig_ref.1, bf16[4,256,256]{2,1,0:T(8,128)(2,1)} %dg_ref.1, f32[1,1024]{1,0:T(1,128)} %bitcast.17, ...), custom_call_target="tpu_custom_call" | custom-call | tf_op jit(solution)/shard_map/layer/pallas_call | solution.py:580
  105.5 1.9 %copy.25 = bf16[64,4096]{1,0:T(8,128)(2,1)} copy(bf16[64,4096]{1,0:T(8,128)(2,1)} %get-tuple-element.4) | data formatting | bytes 1048576
  107.4 1.9 %copy.26 = bf16[64,4096]{1,0:T(8,128)(2,1)} copy(bf16[64,4096]{1,0:T(8,128)(2,1)} %get-tuple-element.5) | data formatting | bytes 1048576

commit v2 on v1

--- a/solution.py
+++ b/solution.py
@@ -171,13 +171,13 @@
             return remote(r_buf.at[q], r_near, r_s.at[j], r_r.at[j], me, q)
         return remote(r_out.at[q], r_in.at[t], r_s.at[j], r_r.at[j], me, q)
 
-    def normalize(ref, gain):
+    def normalize(ref, gain, first):
         def some(r, _):
-            at = pl.ds(pl.multiple_of(r * 16, 16), 16)
+            at = pl.ds(pl.multiple_of(first + r * 32, 16), 32)
             ref[at, :] = rms_scale(ref[at, :], gain[...]).astype(bf16)
             return 0
 
-        lax.fori_loop(0, ref.shape[0] // 16, some, 0)
+        lax.fori_loop(0, rows // 32, some, 0)
 
     halo_copy().start()
     member = lax.broadcasted_iota(jnp.int32, (ep, rows), 0)
@@ -210,7 +210,7 @@
     wd_load.start()
     sd_load = load(sd_hbm, sd, 5)
     sd_load.start()
-    normalize(en, xg_ref)
+    normalize(en, xg_ref, 0)
     mine = pl.ds(pl.multiple_of(t * dq, dq), dq)
 
     def place(i):
@@ -239,17 +239,25 @@
         def _():
             lax.fori_loop(lo, hi, dispatch_far, 0)
 
-    lax.fori_loop(1, 2, dispatch_near, 0)
-    dispatch_fars(1, 0, quarter + 1)
-    lax.fori_loop(2, half - 1, dispatch_near, 0)
+    def dispatch_nears(when, lo, hi):
+        @pl.when(inner == when)
+        def _():
+            lax.fori_loop(lo, hi, dispatch_near, 0)
+
+    lax.fori_loop(1, quarter, dispatch_near, 0)
+    dispatch_fars(1, 0, quarter)
+    lax.fori_loop(quarter, half - 1, dispatch_near, 0)
     local = place(0)
     for q in range(tp):
         recv[q, 0] = jnp.dot(
             local, en[:, pl.ds(q * dq, dq)], preferred_element_type=f32
         ).astype(bf16)
     rows_load.wait()
+    normalize(normed, mg_ref, halo_rows)
     halo_copy().wait_recv()
-    normalize(normed, mg_ref)
+    normed[pl.ds(0, halo_rows), :] = rms_scale(
+        normed[pl.ds(0, halo_rows), :], mg_ref[...]
+    ).astype(bf16)
     sg_load = load(sg_hbm, w1.at[:, pl.ds(0, sh_width)], 6)
     su_load = load(su_hbm, w1.at[:, pl.ds(sh_width, sh_width)], 7)
     gp_load = load(gp_hbm, w1, 8)
@@ -445,44 +453,44 @@
 
     first_far = groups // 2
     project()
+    dispatch_fars(1, quarter, half)
+    dispatch_nears(0, half - 1, half)
     convolve()
     scan()
-    lax.fori_loop(half - 1, half, dispatch_near, 0)
-    dispatch_fars(1, quarter + 1, half)
-    dispatch_fars(0, 0, half)
     gate_step()
+    dispatch_nears(1, half - 1, half)
+    dispatch_fars(0, 0, quarter)
+    arrive(first_far)
+    shared()
+    dispatch_fars(0, quarter, half)
+    arrive(0)
     eg_load.wait()
     eu_load.wait()
-    arrive(0)
-    arrive(first_far)
     feed(0)
-    shared()
+    forward(first_far)
+    feed(first_far)
     for g in range(1, first_far):
         arrive(g)
         feed(g)
-    carry_in()
-    project_out()
     wd_load.wait()
     for i in range(1, tp):
         w_copy(i).wait()
-    forward(first_far)
-    feed(first_far)
-    pass_on(0)
-    finish(0)
     for g in range(first_far + 1, groups):
-        arrive(g)
         pass_on(g - 1)
         finish(g - 1)
+        arrive(g)
         if g == first_far + 1:
-            for near in range(1, first_far):
+            for near in range(first_far):
                 pass_on(near)
                 finish(near)
         forward(g)
         feed(g)
     shared_half()
-    mixer_half()
+    carry_in()
+    project_out()
     pass_on(groups - 1)
     finish(groups - 1)
+    mixer_half()
 
     def combine(lo, count):
         flat = back[pl.ds(lo, count)].reshape(count * cap, dq)

time: 109 us -> 104 us (0.954)
  Pallas kernels: 105 us -> 99.1 us
    pallas_call x1, Pallas kernels: 105 us -> 99.1 us  [layer(): pl.pallas_call(functools.partial(layer_kernel, ep, tp, top), out_shape=[j...]
where the time goes in v2:
time: 104 us; the launch traced here: 103 us
  Pallas kernels  99.1 us (95%)
  local copies, waits for them, and re-layouts  3.74 us (4%)
    pallas_call x1, Pallas kernels, layer(): pl.pallas_call(functools.partial(layer_kernel, ep, tp, top), out_shape=[j...  99.1 us
    unnamed x2, local copies, waits for them, and re-layouts  3.74 us

profile of v2, /device:TPU:1, one launch (start us, length us, event | category | flops | bytes accessed | tf_op | source)
XLA Modules:
  0.0 103.5 jit_solution(4343034383435649695)
XLA Ops:
  0.6 99.1 %layer.1 = (bf16[64,4096]{1,0:T(8,128)(2,1)}, bf16[64,4096]{1,0:T(8,128)(2,1)}) custom-call(s32[2,256]{1,0:T(2,128)} %bitcast.18, f32[2,256]{1,0:T(2,128)} %bitcast.19, f32[4,1024]{1,0:T(4,128)} %taps_ref.1, bf16[4,256,256]{2,1,0:T(8,128)(2,1)} %ig_ref.1, bf16[4,256,256]{2,1,0:T(8,128)(2,1)} %dg_ref.1, f32[1,1024]{1,0:T(1,128)} %bitcast.17, ...), custom_call_target="tpu_custom_call" | custom-call | tf_op jit(solution)/shard_map/layer/pallas_call | solution.py:588
  99.7 1.9 %copy.25 = bf16[64,4096]{1,0:T(8,128)(2,1)} copy(bf16[64,4096]{1,0:T(8,128)(2,1)} %get-tuple-element.4) | data formatting | bytes 1048576
  101.6 1.9 %copy.26 = bf16[64,4096]{1,0:T(8,128)(2,1)} copy(bf16[64,4096]{1,0:T(8,128)(2,1)} %get-tuple-element.5) | data formatting | bytes 1048576

commit v3 on v2

--- a/solution.py
+++ b/solution.py
@@ -35,7 +35,10 @@
     barrier = pltpu.get_barrier_semaphore()
     for ep_at, tp_at in peers:
         pl.semaphore_signal(barrier, inc=1, device_id=(ep_at, tp_at), device_id_type=MESH)
-    pl.semaphore_wait(barrier, len(peers))
+
+
+def meet(count):
+    pl.semaphore_wait(pltpu.get_barrier_semaphore(), count)
 
 
 def expm1_neg(y):
@@ -51,16 +54,24 @@
 
 def layer_kernel(
     ep, tp, top,
-    ids_ref, weights_ref, taps_ref, ig_ref, dg_ref, offset_ref, mg_ref, xg_ref, ms_ref, es_ref,
+    count, *refs,
+):
+    small_hbm, large, small = refs[:count], refs[count:-count], refs[-count:]
+    layer_body(ep, tp, top, small_hbm, small, *large)
+
+
+def layer_body(
+    ep, tp, top, small_hbm, small,
     rows_hbm, tokens_hbm, ip_hbm, gp_hbm, op_hbm, eg_hbm, eu_hbm, ed, sg_hbm, su_hbm, sd_hbm,
-    mo_ref, eo_ref,
+    mo_hbm, eo_hbm,
     outq, normed, en, e_out, r_out, r_near,
     w1, eg, eu, wd, sd, recv, hid, ret, back, mt, st, m_half, e_half, m_out, m_in, e_in,
-    r_buf, r_in, total, gate, a_buf, b_buf, ext, ends, got, gated, meta, cols_ref,
-    load_sem, halo_send, halo_recv, end_send, end_recv,
+    r_buf, r_in, total, gate, a_buf, b_buf, ext, ends, got, gated, meta, cols_ref, mo_ref, eo_ref,
+    load_sem, small_sem, out_sem, halo_send, halo_recv, end_send, end_recv,
     z_s, z_r, y_s, y_r, c_s, c_r, hy_s, hy_r, hc_s, hc_r, w_s, w_r, b_s, b_r,
-    md_s, md_r, ed_s, ed_r, my_s, my_r, ey_s, ey_r, r_s, r_r,
+    md_s, md_r, ed_s, ed_r, my_s, my_r, ey_s, ey_r, r_s, r_r, l_s, l_r,
 ):
+    ids_ref, weights_ref, xg_ref, taps_ref, ig_ref, dg_ref, offset_ref, mg_ref, ms_ref, es_ref = small
     me, t = lax.axis_index("ep"), lax.axis_index("tp")
     ys = tp // 2
     y, c = t // 2, lax.rem(t, 2)
@@ -72,7 +83,8 @@
     blocks, bw = ig_ref.shape[0], ig_ref.shape[1]
     sh_width = sd.shape[0]
     half, quarter = ep // 2, ep // 4
-    groups = ep // 2
+    sizes = [2] * quarter + [1] * half
+    groups, first_far = quarter + half, quarter
     inner = lax.rem(me // quarter + 1, 4) // 2
 
     def at_y(k):
@@ -95,57 +107,64 @@
         return half + lax.rem(j + inner * quarter, half)
 
     def base_of(g):
-        return 2 * g if 2 * g < half else far(2 * g - half)
+        start = sum(sizes[:g])
+        return start if start < half else far(start - half)
+
+    def span_of(g):
+        return pl.ds(base_of(g), sizes[g])
 
     def blocks_of(g):
-        base = base_of(g)
-        return [i for i in (base, base + 1) if not (isinstance(i, int) and i == 0)]
+        return [base_of(g) + n for n in range(sizes[g]) if g + n > 0]
 
     def load(src, dst, at):
         return pltpu.make_async_copy(src, dst, load_sem.at[at])
 
+    peers = [(lax.rem(me + i, ep), t) for i in range(1, ep)] + [
+        (me, lax.rem(t + i, tp)) for i in range(1, tp)
+    ]
+    greet(peers)
+    small_loads = [
+        pltpu.make_async_copy(src, dst, small_sem.at[n])
+        for n, (src, dst) in enumerate(zip(small_hbm, small))
+    ]
     tokens_load, rows_load = load(tokens_hbm, en, 0), load(
         rows_hbm, normed.at[pl.ds(halo_rows, rows)], 9 + tp
     )
+    ip_load = load(ip_hbm, w1, 1)
     tokens_load.start()
-    rows_load.start()
-    ip_load = load(ip_hbm, w1, 1)
-    ip_load.start()
-
-    greet(
-        [(lax.rem(me + i, ep), t) for i in range(1, ep)]
-        + [(me, lax.rem(t + i, tp)) for i in range(1, tp)]
-    )
-
-    def z_copy(i, yy):
-        return remote(
-            outq.at[yy, i], recv.at[yy * 2 + c, i], z_s.at[yy, i], z_r.at[yy, i], partner(i), t
-        )
+    for one in small_loads[:3]:
+        one.start()
+
+    def z_copy(i, yy, near):
+        n = yy * half + i if near else ys * half - half + i
+        return remote(outq.at[yy, i], recv.at[yy * 2 + c, i], z_s.at[n], z_r.at[n], partner(i), t)
 
     def y_copy(k, i):
-        return remote(recv.at[t, i], recv.at[t, i], y_s.at[k, i], y_r.at[k, i], me, up(k))
+        n = i - half
+        part = recv.at[t, i]
+        return remote(part, part, y_s.at[k - 1, n], y_r.at[k - 1, n], me, up(k))
 
     def c_copy(k, i):
         q = down_of(k, c)
-        return remote(recv.at[q, i], recv.at[q, i], c_s.at[k, i], c_r.at[k, i], me, mate)
+        return remote(recv.at[q, i], recv.at[q, i], c_s.at[k, i - 1], c_r.at[k, i - 1], me, mate)
 
     def hy_copy(k, g):
-        part = hid.at[t, pl.ds(base_of(g), 2)]
-        return remote(part, part, hy_s.at[k, g], hy_r.at[k, g], me, up(k))
+        part = hid.at[t, span_of(g)]
+        return remote(part, part, hy_s.at[k - 1, g], hy_r.at[k - 1, g], me, up(k))
 
     def hc_copy(k, g):
-        part = hid.at[down_of(k, c), pl.ds(base_of(g), 2)]
+        part = hid.at[down_of(k, c), span_of(g)]
         return remote(part, part, hc_s.at[k, g], hc_r.at[k, g], me, mate)
 
     def w_copy(i):
         q = lax.rem(t + i, tp)
         return remote(
             ed.at[:, pl.ds(pl.multiple_of(q * dq, dq), dq)], wd.at[t],
-            w_s.at[i], w_r.at[i], me, q,
+            w_s.at[i - 1], w_r.at[i - 1], me, q,
         )
 
     def b_copy(i):
-        return remote(ret.at[i], back.at[i], b_s.at[i], b_r.at[i], partner(i), t)
+        return remote(ret.at[i], back.at[i], b_s.at[i - 1], b_r.at[i - 1], partner(i), t)
 
     def halo_copy():
         return remote(
@@ -154,22 +173,31 @@
         )
 
     def end_copy(i):
-        return remote(ends, got.at[i], end_send.at[i], end_recv.at[i], lax.rem(me + i, ep), t)
+        n, to = i - 1, lax.rem(me + i, ep)
+        return remote(ends, got.at[i], end_send.at[n], end_recv.at[n], to, t)
 
     def pair(ref, half, s, r, k):
         return remote(ref.at[at_y(k) * 2 + 1 - c], half.at[k], s.at[k], r.at[k], me, mate)
 
     def my_copy(k):
-        return remote(m_out.at[k], m_in.at[k], my_s.at[k], my_r.at[k], me, up(k))
-
-    def ey_copy(k):
-        return remote(e_out.at[k], e_in.at[k], ey_s.at[k], ey_r.at[k], me, up(k))
-
-    def r_copy(k, core):
-        j, q = 2 * k + core, at_y(k) * 2 + lax.rem(c + core, 2)
-        if k == 0:
-            return remote(r_buf.at[q], r_near, r_s.at[j], r_r.at[j], me, q)
-        return remote(r_out.at[q], r_in.at[t], r_s.at[j], r_r.at[j], me, q)
+        return remote(m_out.at[k], m_in.at[k], my_s.at[k - 1], my_r.at[k - 1], me, up(k))
+
+    def ey_copy(k, j):
+        s, r = ey_s.at[k - 1, j - 1], ey_r.at[k - 1, j - 1]
+        return remote(e_out.at[k, j], e_in.at[k, j], s, r, me, up(k))
+
+    def r_copy(k):
+        return remote(r_buf.at[at_y(k) * 2 + 1 - c], r_near.at[k], r_s.at[k], r_r.at[k], me, mate)
+
+    def late_copy(k, j):
+        s, r = l_s.at[k - 1, j], l_r.at[k - 1, j]
+        return remote(r_out.at[k, j], r_in.at[k, j], s, r, me, up(k))
+
+    def of_chip(yy):
+        return pl.ds(pl.multiple_of(yy * 2 * dq, dq), 2 * dq)
+
+    def of_core(yy, core):
+        return pl.ds(pl.multiple_of((yy * 2 + core) * dq, dq), dq)
 
     def normalize(ref, gain, first):
         def some(r, _):
@@ -179,7 +207,8 @@
 
         lax.fori_loop(0, rows // 32, some, 0)
 
-    halo_copy().start()
+    for one in small_loads[:3]:
+        one.wait()
     member = lax.broadcasted_iota(jnp.int32, (ep, rows), 0)
     chosen = [
         (jnp.bitwise_xor(ids_ref[k : k + 1, :], me) == member).astype(f32) for k in range(top)
@@ -201,6 +230,13 @@
     cols_ref[...] = meta[...].T
 
     tokens_load.wait()
+    rows_load.start()
+    for one in small_loads[3:]:
+        one.start()
+    ip_load.start()
+    normalize(en, xg_ref, 0)
+    meet(len(peers))
+    halo_copy().start()
     for i in range(1, tp):
         w_copy(i).start()
     eg_load, eu_load = load(eg_hbm, eg, 2), load(eu_hbm, eu, 3)
@@ -210,7 +246,6 @@
     wd_load.start()
     sd_load = load(sd_hbm, sd, 5)
     sd_load.start()
-    normalize(en, xg_ref, 0)
     mine = pl.ds(pl.multiple_of(t * dq, dq), dq)
 
     def place(i):
@@ -225,13 +260,13 @@
         for yy in range(ys):
             part = pl.ds(pl.multiple_of((yy * 2 + c) * dq, dq), dq)
             outq[yy, i] = jnp.dot(hot, en[:, part], preferred_element_type=f32).astype(bf16)
-            z_copy(i, yy).start()
+            z_copy(i, yy, True).start()
         return 0
 
     def dispatch_far(j, _):
         i = far(j)
         outq[y, i] = jnp.dot(place(i), en[:, mine], preferred_element_type=f32).astype(bf16)
-        z_copy(i, y).start()
+        z_copy(i, y, False).start()
         return 0
 
     def dispatch_fars(when, lo, hi):
@@ -252,6 +287,9 @@
         recv[q, 0] = jnp.dot(
             local, en[:, pl.ds(q * dq, dq)], preferred_element_type=f32
         ).astype(bf16)
+    dispatch_fars(1, quarter, half - 1)
+    for one in small_loads[3:]:
+        one.wait()
     rows_load.wait()
     normalize(normed, mg_ref, halo_rows)
     halo_copy().wait_recv()
@@ -376,14 +414,14 @@
                 gated[...], w1[pl.ds(q * width, width), :], preferred_element_type=f32
             )
             mt[:, :, pl.ds(q * dq, dq)] = piece.reshape(tp, each, dq)
-        for k in range(ys):
-            pair(mt, m_half, md_s, md_r, k).start()
 
     def shared_half():
         for k in range(1, ys):
             pair(st, e_half, ed_s, ed_r, k).wait_recv()
-            e_out[k] = (e_half[k] + st[up(k)]).astype(bf16)
-            ey_copy(k).start()
+            for j in range(1, ys):
+                cols = of_chip(at_y(j))
+                e_out[k, j] = (e_half[k, :, cols] + st[up(k), :, cols]).astype(bf16)
+                ey_copy(k, j).start()
 
     def mixer_half():
         for k in range(1, ys):
@@ -393,19 +431,19 @@
 
     def arrive(g):
         for i in blocks_of(g):
-            if 2 * g < half:
+            if g < first_far:
                 for yy in range(ys):
-                    z_copy(i, yy).wait_recv()
+                    z_copy(i, yy, True).wait_recv()
                 for k in range(ys):
                     c_copy(k, i).start()
             else:
-                z_copy(i, y).wait_recv()
+                z_copy(i, y, False).wait_recv()
                 for k in range(1, ys):
                     y_copy(k, i).start()
                 c_copy(0, i).start()
 
     def forward(g):
-        if 2 * g >= half:
+        if g >= first_far:
             for i in blocks_of(g):
                 for k in range(1, ys):
                     y_copy(k, i).wait_recv()
@@ -415,17 +453,17 @@
         for i in blocks_of(g):
             for k in range(ys):
                 c_copy(k, i).wait_recv()
-        both = pl.ds(base_of(g), 2)
+        both = span_of(g)
         gate_sum = up_sum = None
         for q in range(tp):
-            x = recv[q, both].reshape(2 * cap, dq)
+            x = recv[q, both].reshape(sizes[g] * cap, dq)
             span = pl.ds(q * dq, dq)
             g_part = jnp.dot(x, eg[span, :], preferred_element_type=f32)
             u_part = jnp.dot(x, eu[span, :], preferred_element_type=f32)
             gate_sum = g_part if gate_sum is None else gate_sum + g_part
             up_sum = u_part if up_sum is None else up_sum + u_part
         hidden = (jax.nn.silu(gate_sum) * up_sum).astype(bf16)
-        hid[t, both] = hidden.reshape(2, cap, hidden.shape[1])
+        hid[t, both] = hidden.reshape(sizes[g], cap, hidden.shape[1])
         for k in range(1, ys):
             hy_copy(k, g).start()
         hc_copy(0, g).start()
@@ -438,22 +476,21 @@
     def finish(g):
         for k in range(ys):
             hc_copy(k, g).wait_recv()
-        both = pl.ds(base_of(g), 2)
+        both = span_of(g)
         out = None
         for q in range(tp):
-            h = hid[q, both].reshape(2 * cap, hid.shape[3])
+            h = hid[q, both].reshape(sizes[g] * cap, hid.shape[3])
             part = jnp.dot(h, wd[q], preferred_element_type=f32)
             out = part if out is None else out + part
-        out = out.astype(bf16).reshape(2, cap, dq)
+        out = out.astype(bf16).reshape(sizes[g], cap, dq)
         if g == 0:
             back[0] = out[0]
         ret[both] = out
         for i in blocks_of(g):
             b_copy(i).start()
 
-    first_far = groups // 2
     project()
-    dispatch_fars(1, quarter, half)
+    dispatch_fars(1, half - 1, half)
     dispatch_nears(0, half - 1, half)
     convolve()
     scan()
@@ -463,33 +500,50 @@
     arrive(first_far)
     shared()
     dispatch_fars(0, quarter, half)
+    arrive(first_far + 1)
     arrive(0)
     eg_load.wait()
     eu_load.wait()
     feed(0)
-    forward(first_far)
-    feed(first_far)
+    wd_load.wait()
+    for g in (first_far, first_far + 1):
+        forward(g)
+        feed(g)
+    for i in range(1, tp):
+        w_copy(i).wait()
+    for g in (first_far, first_far + 1):
+        pass_on(g)
+        finish(g)
     for g in range(1, first_far):
         arrive(g)
         feed(g)
-    wd_load.wait()
-    for i in range(1, tp):
-        w_copy(i).wait()
-    for g in range(first_far + 1, groups):
-        pass_on(g - 1)
-        finish(g - 1)
+    last = groups - 2
+    for g in range(first_far + 2, last):
         arrive(g)
-        if g == first_far + 1:
-            for near in range(first_far):
-                pass_on(near)
-                finish(near)
         forward(g)
         feed(g)
+        pass_on(g)
+        finish(g)
+    arrive(last)
+    pass_on(0)
+    finish(0)
+    arrive(last + 1)
+    for near in range(1, first_far):
+        pass_on(near)
+        finish(near)
+    forward(last)
+    feed(last)
+    forward(last + 1)
+    feed(last + 1)
+    pass_on(last)
+    finish(last)
     shared_half()
     carry_in()
     project_out()
-    pass_on(groups - 1)
-    finish(groups - 1)
+    pass_on(last + 1)
+    for k in range(ys):
+        pair(mt, m_half, md_s, md_r, k).start()
+    finish(last + 1)
     mixer_half()
 
     def combine(lo, count):
@@ -508,48 +562,55 @@
         b_copy(i).wait_recv()
     r_buf[...] = combine(0, half)
     pair(st, e_half, ed_s, ed_r, 0).wait_recv()
-    whole = e_half[0] + st[t]
+    total[...] = e_half[0] + st[t]
     for k in range(1, ys):
-        ey_copy(k).wait_recv()
-        whole = whole + e_in[k].astype(f32)
-    total[...] = whole
+        for j in range(1, ys):
+            ey_copy(k, j).wait_recv()
+            cols = of_chip(lax.rem(y + ys - k + j, ys))
+            total[:, cols] = total[:, cols] + e_in[k, j].astype(f32)
     pair(mt, m_half, md_s, md_r, 0).wait_recv()
     whole = m_half[0] + mt[t]
     for k in range(1, ys):
         my_copy(k).wait_recv()
         whole = whole + m_in[k].astype(f32)
     mo_ref[...] = rms_scale(whole, ms_ref[...]).astype(bf16)
+    mo_store = pltpu.make_async_copy(mo_ref, mo_hbm, out_sem.at[0])
+    mo_store.start()
     for i in range(half, ep):
         b_copy(i).wait_recv()
-    routed = r_buf[...] + combine(half, half)
-    r_out[...] = routed.astype(bf16)
+    r_buf[...] = r_buf[...] + combine(half, half)
+    for k in range(ys):
+        r_copy(k).start()
+    near = of_core(y, 1 - c)
     for k in range(1, ys):
-        for core in range(2):
-            r_copy(k, core).start()
-    r_buf[...] = routed
-    r_copy(0, 1).start()
+        r_out[k, 0] = (e_half[k, :, mine] + st[up(k), :, mine] + r_buf[up(k)]).astype(bf16)
+        late_copy(k, 0).start()
+    for k in range(1, ys):
+        r_copy(k).wait_recv()
+        r_out[k, 1] = (e_half[k, :, near] + st[up(k), :, near] + r_near[k]).astype(bf16)
+        late_copy(k, 1).start()
     total[:, mine] = total[:, mine] + r_buf[t]
-    r_copy(0, 1).wait()
-    near = pl.ds(pl.multiple_of(mate * dq, dq), dq)
-    total[:, near] = total[:, near] + r_near[...]
+    r_copy(0).wait_recv()
+    total[:, near] = total[:, near] + r_near[0]
     for k in range(1, ys):
-        for core in range(2):
-            r_copy(k, core).wait()
-            q = down_of(k, lax.rem(c + core, 2))
-            cols = pl.ds(pl.multiple_of(q * dq, dq), dq)
-            total[:, cols] = total[:, cols] + r_in[q].astype(f32)
+        for j in range(2):
+            late_copy(k, j).wait_recv()
+            cols = of_core(lax.rem(y + ys - k, ys), lax.rem(c + j, 2))
+            total[:, cols] = total[:, cols] + r_in[k, j].astype(f32)
     eo_ref[...] = rms_scale(total[...], es_ref[...]).astype(bf16)
+    eo_store = pltpu.make_async_copy(eo_ref, eo_hbm, out_sem.at[1])
+    eo_store.start()
 
     def settle_near(i, _):
         for yy in range(ys):
-            z_copy(i, yy).wait_send()
+            z_copy(i, yy, True).wait_send()
         for k in range(ys):
             c_copy(k, i).wait_send()
         b_copy(i).wait_send()
         return 0
 
     def settle_far(i, _):
-        z_copy(i, y).wait_send()
+        z_copy(i, y, False).wait_send()
         for k in range(1, ys):
             y_copy(k, i).wait_send()
         for k in range(ys):
@@ -568,9 +629,16 @@
     for k in range(ys):
         pair(mt, m_half, md_s, md_r, k).wait_send()
         pair(st, e_half, ed_s, ed_r, k).wait_send()
+    for k in range(ys):
+        r_copy(k).wait_send()
     for k in range(1, ys):
         my_copy(k).wait_send()
-        ey_copy(k).wait_send()
+        for j in range(1, ys):
+            ey_copy(k, j).wait_send()
+        for j in range(2):
+            late_copy(k, j).wait_send()
+    mo_store.wait()
+    eo_store.wait()
 
 
 def dma(*shape):
@@ -583,21 +651,21 @@
     hf, hs = large[5].shape[1], large[8].shape[1]
     top = small[0].shape[0]
     each, ys, dq = rows // tp, tp // 2, depth // tp
+    groups = ep // 4 + ep // 2
     cap = rows * top * 3 // (2 * ep)
     V = pltpu.VMEM
     return pl.pallas_call(
-        functools.partial(layer_kernel, ep, tp, top),
+        functools.partial(layer_kernel, ep, tp, top, len(small)),
         out_shape=[jax.ShapeDtypeStruct((each, depth), bf16)] * 2,
-        in_specs=[pl.BlockSpec(memory_space=V)] * len(small)
-        + [pl.BlockSpec(memory_space=pl.ANY)] * len(large),
-        out_specs=[pl.BlockSpec(memory_space=V)] * 2,
+        in_specs=[pl.BlockSpec(memory_space=pl.ANY)] * (len(small) + len(large)),
+        out_specs=[pl.BlockSpec(memory_space=pl.ANY)] * 2,
         scratch_shapes=[
             V((ys, ep, cap, dq), bf16),
             V((halo_rows + rows, depth), bf16),
             V((rows, depth), bf16),
-            V((ys, each, depth), bf16),
-            V((tp, each, dq), bf16),
-            V((each, dq), f32),
+            V((ys, ys, each, 2 * dq), bf16),
+            V((ys, 2, each, dq), bf16),
+            V((ys, each, dq), f32),
             V((depth, width), bf16),
             V((depth, hf), bf16),
             V((depth, hf), bf16),
@@ -613,9 +681,9 @@
             V((ys, each, depth), f32),
             V((ys, each, depth), bf16),
             V((ys, each, depth), bf16),
-            V((ys, each, depth), bf16),
+            V((ys, ys, each, 2 * dq), bf16),
             V((tp, each, dq), f32),
-            V((tp, each, dq), bf16),
+            V((ys, 2, each, dq), bf16),
             V((each, depth), f32),
             V((rows, width), f32),
             V((rows, width), f32),
@@ -626,23 +694,42 @@
             V((rows, width), bf16),
             V((128, rows), f32),
             V((rows, 128), f32),
-            dma(10 + tp), pltpu.SemaphoreType.DMA, pltpu.SemaphoreType.DMA, dma(ep), dma(ep),
-            dma(ys, ep), dma(ys, ep),
-            dma(ys, ep), dma(ys, ep),
-            dma(ys, ep), dma(ys, ep),
-            dma(ys, ep // 2), dma(ys, ep // 2),
-            dma(ys, ep // 2), dma(ys, ep // 2),
-            dma(tp), dma(tp),
-            dma(ep), dma(ep),
+            V((each, depth), bf16),
+            V((each, depth), bf16),
+            dma(10 + tp), dma(len(small)), dma(2), pltpu.SemaphoreType.DMA, pltpu.SemaphoreType.DMA,
+            dma(ep - 1), dma(ep - 1),
+            dma((ys + 1) * ep // 2), dma((ys + 1) * ep // 2),
+            dma(ys - 1, ep // 2), dma(ys - 1, ep // 2),
+            dma(ys, ep - 1), dma(ys, ep - 1),
+            dma(ys - 1, groups), dma(ys - 1, groups),
+            dma(ys, groups), dma(ys, groups),
+            dma(tp - 1), dma(tp - 1),
+            dma(ep - 1), dma(ep - 1),
             dma(ys), dma(ys), dma(ys), dma(ys),
-            dma(ys), dma(ys), dma(ys), dma(ys),
-            dma(tp), dma(tp),
-        ],
+            dma(ys - 1), dma(ys - 1), dma(ys - 1, ys - 1), dma(ys - 1, ys - 1),
+            dma(ys), dma(ys), dma(ys - 1, 2), dma(ys - 1, 2),
+        ]
+        + [V(x.shape, x.dtype) for x in small],
         compiler_params=pltpu.CompilerParams(
             collective_id=0, has_side_effects=True, vmem_limit_bytes=67000000
         ),
         name="layer",
     )(*small, *large)
+
+
+def publish_kernel(mixer, expert, mixer_out, expert_out):
+    mixer_out[...] = mixer[...]
+    expert_out[...] = expert[...]
+
+
+def publish(mixer, expert):
+    return pl.pallas_call(
+        publish_kernel,
+        out_shape=[jax.ShapeDtypeStruct(x.shape, x.dtype) for x in (mixer, expert)],
+        in_specs=[pl.BlockSpec(memory_space=pltpu.VMEM)] * 2,
+        out_specs=[pl.BlockSpec(memory_space=pltpu.VMEM)] * 2,
+        name="publish",
+    )(mixer, expert)
 
 
 def body(
@@ -653,14 +740,14 @@
     ep, tp = lax.axis_size("ep"), lax.axis_size("tp")
     gains = [x.reshape(1, -1) for x in (mixer_gain, expert_gain, mixer_scale, expert_scale)]
     small = (
-        route_ids.T, route_weights.T, conv_taps, input_gates, decay_gates,
-        decay_offset.reshape(1, -1), *gains,
+        route_ids.T, route_weights.T, gains[1], conv_taps, input_gates, decay_gates,
+        decay_offset.reshape(1, -1), gains[0], gains[2], gains[3],
     )
     large = (
         mixer_rows, expert_rows, input_proj, gate_proj, out_proj, expert_gate[0], expert_up[0], expert_down[0],
         shared_gate, shared_up, shared_down,
     )
-    return tuple(layer(ep, tp, small, large))
+    return tuple(publish(*layer(ep, tp, small, large)))
 
 
 def solution(mesh):

time: 104 us -> 101 us (0.971)
  local copies, waits for them, and re-layouts: 3.74 us -> 0 us
    unnamed x2 -> x0, local copies, waits for them, and re-layouts: 3.74 us -> none
    pallas_call x1 -> x2, Pallas kernels: 99.1 us -> 99.7 us  [the longest x1 97.5 us: layer(): pl.pallas_call(functools.partial(layer_kernel, ep, tp, top, len(small)),...]
where the time goes in v3:
time: 101 us; the launch traced here: 100 us
  Pallas kernels  99.7 us (99%)
    pallas_call x1, Pallas kernels, layer(): pl.pallas_call(functools.partial(layer_kernel, ep, tp, top, len(small)),...  97.5 us
    pallas_call x1, Pallas kernels, publish(): pl.pallas_call(publish_kernel, out_shape=[jax.ShapeDtypeStruct(x.shape, x...  2.2 us

profile of v3, /device:TPU:1, one launch (start us, length us, event | category | flops | bytes accessed | tf_op | source)
XLA Modules:
  0.0 100.4 jit_solution(8145569050222731562)
XLA Ops:
  0.6 97.5 %layer.1 = (bf16[64,4096]{1,0:T(8,128)(2,1)}, bf16[64,4096]{1,0:T(8,128)(2,1)}) custom-call(s32[2,256]{1,0:T(2,128)} %bitcast.18, f32[2,256]{1,0:T(2,128)} %bitcast.19, f32[1,4096]{1,0:T(1,128)} %bitcast.13, f32[4,1024]{1,0:T(4,128)} %refs_3_.1, bf16[4,256,256]{2,1,0:T(8,128)(2,1)} %refs_4_.1, bf16[4,256,256]{2,1,0:T(8,128)(2,1)} %refs_5_.1, ...), custom_call_target="tpu_custom_call" | custom-call | tf_op jit(solution)/shard_map/layer/pallas_call | solution.py:657
  98.2 2.2 %publish.1 = (bf16[64,4096]{1,0:T(8,128)(2,1)}, bf16[64,4096]{1,0:T(8,128)(2,1)}) custom-call(bf16[64,4096]{1,0:T(8,128)(2,1)} %get-tuple-element.4.mixer, bf16[64,4096]{1,0:T(8,128)(2,1)} %get-tuple-element.5.expert), custom_call_target="tpu_custom_call" | custom-call | tf_op jit(solution)/shard_map/publish/pallas_call | solution.py:726

commit v4 on v3

--- a/solution.py
+++ b/solution.py
@@ -166,6 +166,14 @@
     def b_copy(i):
         return remote(ret.at[i], back.at[i], b_s.at[i - 1], b_r.at[i - 1], partner(i), t)
 
+    def side(h):
+        return pl.ds(h * (dq // 2), dq // 2)
+
+    def side_copy(i, h):
+        n, to = (h + 1) * half - 1 + i - half, partner(i)
+        cols = (i, slice(None), side(h))
+        return remote(ret.at[cols], back.at[cols], b_s.at[n], b_r.at[n], to, t)
+
     def halo_copy():
         return remote(
             rows_hbm.at[pl.ds(rows - halo_rows, halo_rows)], normed.at[pl.ds(0, halo_rows)],
@@ -186,12 +194,13 @@
         s, r = ey_s.at[k - 1, j - 1], ey_r.at[k - 1, j - 1]
         return remote(e_out.at[k, j], e_in.at[k, j], s, r, me, up(k))
 
-    def r_copy(k):
-        return remote(r_buf.at[at_y(k) * 2 + 1 - c], r_near.at[k], r_s.at[k], r_r.at[k], me, mate)
-
-    def late_copy(k, j):
-        s, r = l_s.at[k - 1, j], l_r.at[k - 1, j]
-        return remote(r_out.at[k, j], r_in.at[k, j], s, r, me, up(k))
+    def r_copy(k, h):
+        src, dst = r_buf.at[at_y(k) * 2 + 1 - c, :, side(h)], r_near.at[k, :, side(h)]
+        return remote(src, dst, r_s.at[k, h], r_r.at[k, h], me, mate)
+
+    def late_copy(k, j, h):
+        s, r = l_s.at[k - 1, j, h], l_r.at[k - 1, j, h]
+        return remote(r_out.at[k, j, :, side(h)], r_in.at[k, j, :, side(h)], s, r, me, up(k))
 
     def of_chip(yy):
         return pl.ds(pl.multiple_of(yy * 2 * dq, dq), 2 * dq)
@@ -487,7 +496,12 @@
             back[0] = out[0]
         ret[both] = out
         for i in blocks_of(g):
-            b_copy(i).start()
+            if g < first_far:
+                b_copy(i).start()
+            else:
+                side_copy(i, 0).start()
+                if g < groups - 2:
+                    side_copy(i, 1).start()
 
     project()
     dispatch_fars(1, half - 1, half)
@@ -533,21 +547,25 @@
         finish(near)
     forward(last)
     feed(last)
+    carry_in()
+    project_out()
     forward(last + 1)
     feed(last + 1)
     pass_on(last)
     finish(last)
-    shared_half()
-    carry_in()
-    project_out()
     pass_on(last + 1)
     for k in range(ys):
         pair(mt, m_half, md_s, md_r, k).start()
+    shared_half()
     finish(last + 1)
     mixer_half()
-
-    def combine(lo, count):
-        flat = back[pl.ds(lo, count)].reshape(count * cap, dq)
+    for g in (last, last + 1):
+        for i in blocks_of(g):
+            side_copy(i, 0).wait_send()
+            side_copy(i, 1).start()
+
+    def combine(lo, count, cols):
+        flat = back[pl.ds(lo, count), :, cols].reshape(count * cap, -1)
         spot = (lax.broadcasted_iota(jnp.int32, (rows, count * cap), 1) + lo * cap).astype(f32)
         out = None
         for k in range(top):
@@ -556,11 +574,11 @@
                 pick, flat, preferred_element_type=f32
             )
             out = term if out is None else out + term
-        return out.reshape(tp, each, dq)
+        return out.reshape(tp, each, -1)
 
     for i in range(1, half):
         b_copy(i).wait_recv()
-    r_buf[...] = combine(0, half)
+    r_buf[...] = combine(0, half, pl.ds(0, dq))
     pair(st, e_half, ed_s, ed_r, 0).wait_recv()
     total[...] = e_half[0] + st[t]
     for k in range(1, ys):
@@ -568,6 +586,29 @@
             ey_copy(k, j).wait_recv()
             cols = of_chip(lax.rem(y + ys - k + j, ys))
             total[:, cols] = total[:, cols] + e_in[k, j].astype(f32)
+    near = of_core(y, 1 - c)
+
+    def part_of(q, h):
+        return pl.ds(pl.multiple_of(q * dq + h * dq // 2, dq // 2), dq // 2)
+
+    for h in range(2):
+        cols, mine_h, near_h = side(h), part_of(t, h), part_of(mate, h)
+        for i in range(half, ep):
+            side_copy(i, h).wait_recv()
+        r_buf[:, :, cols] = r_buf[:, :, cols] + combine(half, half, cols)
+        for k in range(ys):
+            r_copy(k, h).start()
+        for k in range(1, ys):
+            r_out[k, 0, :, cols] = (
+                e_half[k, :, mine_h] + st[up(k), :, mine_h] + r_buf[up(k), :, cols]
+            ).astype(bf16)
+            late_copy(k, 0, h).start()
+        for k in range(1, ys):
+            r_copy(k, h).wait_recv()
+            r_out[k, 1, :, cols] = (
+                e_half[k, :, near_h] + st[up(k), :, near_h] + r_near[k, :, cols]
+            ).astype(bf16)
+            late_copy(k, 1, h).start()
     pair(mt, m_half, md_s, md_r, 0).wait_recv()
     whole = m_half[0] + mt[t]
     for k in range(1, ys):
@@ -576,25 +617,14 @@
     mo_ref[...] = rms_scale(whole, ms_ref[...]).astype(bf16)
     mo_store = pltpu.make_async_copy(mo_ref, mo_hbm, out_sem.at[0])
     mo_store.start()
-    for i in range(half, ep):
-        b_copy(i).wait_recv()
-    r_buf[...] = r_buf[...] + combine(half, half)
-    for k in range(ys):
-        r_copy(k).start()
-    near = of_core(y, 1 - c)
-    for k in range(1, ys):
-        r_out[k, 0] = (e_half[k, :, mine] + st[up(k), :, mine] + r_buf[up(k)]).astype(bf16)
-        late_copy(k, 0).start()
-    for k in range(1, ys):
-        r_copy(k).wait_recv()
-        r_out[k, 1] = (e_half[k, :, near] + st[up(k), :, near] + r_near[k]).astype(bf16)
-        late_copy(k, 1).start()
     total[:, mine] = total[:, mine] + r_buf[t]
-    r_copy(0).wait_recv()
+    for h in range(2):
+        r_copy(0, h).wait_recv()
     total[:, near] = total[:, near] + r_near[0]
     for k in range(1, ys):
         for j in range(2):
-            late_copy(k, j).wait_recv()
+            for h in range(2):
+                late_copy(k, j, h).wait_recv()
             cols = of_core(lax.rem(y + ys - k, ys), lax.rem(c + j, 2))
             total[:, cols] = total[:, cols] + r_in[k, j].astype(f32)
     eo_ref[...] = rms_scale(total[...], es_ref[...]).astype(bf16)
@@ -615,9 +645,13 @@
             y_copy(k, i).wait_send()
         for k in range(ys):
             c_copy(k, i).wait_send()
-        b_copy(i).wait_send()
         return 0
 
+    for g in range(first_far, groups):
+        for i in blocks_of(g):
+            if g < groups - 2:
+                side_copy(i, 0).wait_send()
+            side_copy(i, 1).wait_send()
     halo_copy().wait_send()
     lax.fori_loop(1, half, settle_near, 0)
     lax.fori_loop(half, ep, settle_far, 0)
@@ -630,13 +664,15 @@
         pair(mt, m_half, md_s, md_r, k).wait_send()
         pair(st, e_half, ed_s, ed_r, k).wait_send()
     for k in range(ys):
-        r_copy(k).wait_send()
+        for h in range(2):
+            r_copy(k, h).wait_send()
     for k in range(1, ys):
         my_copy(k).wait_send()
         for j in range(1, ys):
             ey_copy(k, j).wait_send()
         for j in range(2):
-            late_copy(k, j).wait_send()
+            for h in range(2):
+                late_copy(k, j, h).wait_send()
     mo_store.wait()
     eo_store.wait()
 
@@ -704,10 +740,10 @@
             dma(ys - 1, groups), dma(ys - 1, groups),
             dma(ys, groups), dma(ys, groups),
             dma(tp - 1), dma(tp - 1),
-            dma(ep - 1), dma(ep - 1),
+            dma(ep + ep // 2 - 1), dma(ep + ep // 2 - 1),
             dma(ys), dma(ys), dma(ys), dma(ys),
             dma(ys - 1), dma(ys - 1), dma(ys - 1, ys - 1), dma(ys - 1, ys - 1),
-            dma(ys), dma(ys), dma(ys - 1, 2), dma(ys - 1, 2),
+            dma(ys, 2), dma(ys, 2), dma(ys - 1, 2, 2), dma(ys - 1, 2, 2),
         ]
         + [V(x.shape, x.dtype) for x in small],
         compiler_params=pltpu.CompilerParams(

time: 101 us -> 99 us (0.980)
  Pallas kernels: 99.7 us -> 97.7 us
    pallas_call x1, Pallas kernels: 97.5 us -> 95.5 us  [layer(): pl.pallas_call(functools.partial(layer_kernel, ep, tp, top, len(small)),...]
where the time goes in v4:
time: 99 us; the launch traced here: 98.3 us
  Pallas kernels  97.7 us (99%)
    pallas_call x1, Pallas kernels, layer(): pl.pallas_call(functools.partial(layer_kernel, ep, tp, top, len(small)),...  95.5 us
    pallas_call x1, Pallas kernels, publish(): pl.pallas_call(publish_kernel, out_shape=[jax.ShapeDtypeStruct(x.shape, x...  2.2 us

profile of v4, /device:TPU:1, one launch (start us, length us, event | category | flops | bytes accessed | tf_op | source)
XLA Modules:
  0.0 98.3 jit_solution(17140459550775254979)
XLA Ops:
  0.6 95.5 %layer.1 = (bf16[64,4096]{1,0:T(8,128)(2,1)}, bf16[64,4096]{1,0:T(8,128)(2,1)}) custom-call(s32[2,256]{1,0:T(2,128)} %bitcast.18, f32[2,256]{1,0:T(2,128)} %bitcast.19, f32[1,4096]{1,0:T(1,128)} %bitcast.13, f32[4,1024]{1,0:T(4,128)} %refs_3_.1, bf16[4,256,256]{2,1,0:T(8,128)(2,1)} %refs_4_.1, bf16[4,256,256]{2,1,0:T(8,128)(2,1)} %refs_5_.1, ...), custom_call_target="tpu_custom_call" | custom-call | tf_op jit(solution)/shard_map/layer/pallas_call | solution.py:693
  96.1 2.2 %publish.1 = (bf16[64,4096]{1,0:T(8,128)(2,1)}, bf16[64,4096]{1,0:T(8,128)(2,1)}) custom-call(bf16[64,4096]{1,0:T(8,128)(2,1)} %get-tuple-element.4.mixer, bf16[64,4096]{1,0:T(8,128)(2,1)} %get-tuple-element.5.expert), custom_call_target="tpu_custom_call" | custom-call | tf_op jit(solution)/shard_map/publish/pallas_call | solution.py:762
